TPU v7x, 32 devices: a whole 2x2x4 slice. The times are simulated.
32 devices in a mesh: row: 4 (over z), col: 8 (over y, x, core).
Axes of the slice: x: 2, y: 2, z: 4, core: 2. Of those that a mesh axis runs over, the one named last changes fastest.
Arguments:
- tokens: bfloat16 [32, 144, 2048], P('row', 'col'), may hold values from -6 to 6
- norm_gain: bfloat16 [2048], replicated, may hold values from 0.099609375 to 1.8984375
- w_in: bfloat16 [2048, 1152], replicated, may hold values from -0.125 to 0.125
- w_out: bfloat16 [1152, 2048], replicated, may hold values from -0.1875 to 0.1875
Outputs:
- mixed: bfloat16 [144, 32, 2048], P('row', 'col')
All inputs are finite; a program needn't handle non-finite values.
Results may differ from a plain program's by a relative error of at most 0.013.
Values may be sent and summed in bfloat16 or wider, within the bound.
A program may use at most 64 MiB of HBM per device.

v0:
```python
import functools
import math

import jax
import jax.numpy as jnp
import numpy as np
from jax import lax
from jax.experimental import pallas as pl
from jax.experimental.pallas import tpu as pltpu
from jax.sharding import PartitionSpec as P

GROUP = 128
LANES = 128
SUBLANES = 16
MESH = pl.DeviceIdType.MESH


norm_eps = 1e-06
highest = lax.Precision.HIGHEST


def folded_list(length_first, devices):
    block = length_first // devices
    half = block // 2
    result = np.zeros(length_first, np.int64)
    for device in range(devices):
        for inner in range(block):
            if inner < half:
                value = device * half + inner
            elif device == 0 and inner == half:
                value = length_first // 2
            else:
                value = length_first - device * half - (inner - half)
            result[device * block + inner] = value % length_first
    return result


def channel_tables(row_count):
    width = GROUP // row_count
    half = width // 2
    per_tile = LANES // width
    j = np.arange(GROUP)
    forward = np.zeros((row_count, per_tile * GROUP, LANES))
    back = np.zeros((row_count, LANES, per_tile * GROUP))
    for row in range(row_count):
        for x in range(width):
            m = row * half + x % half
            cosine = x < half
            column = np.cos(2 * np.pi * j * m / GROUP) if cosine else np.sin(2 * np.pi * j * m / GROUP)
            entries = [(m, 1.0)]
            if not cosine and m == 0:
                column = np.cos(np.pi * j)
                entries = [(GROUP // 2, 1.0)]
            elif m:
                entries = [(m, 1.0 if cosine else -1.0), (GROUP - m, 1.0)]
            for g in range(per_tile):
                forward[row, g * GROUP : (g + 1) * GROUP, g * width + x] = column
                for at, sign in entries:
                    back[row, g * width + x, g * GROUP + at] = sign
    return forward, back


def position_tables(rows_first, rows_second, row_count, col_count, chunk, chunks):
    length_first = rows_first * row_count
    length_second = rows_second * col_count
    positions = length_first * length_second
    block = length_first // col_count
    half = block // 2
    a = np.arange(length_first)
    first = np.zeros((col_count, chunks, col_count, block, chunk, row_count, chunk, rows_first))
    for col in range(col_count):
        for i in range(rows_second):
            at, j = divmod(i, chunk)
            p = a * length_second + col * rows_second + i
            for target in range(col_count):
                for f_at in range(half):
                    f = target * half + f_at
                    angle = 2 * np.pi * (f * p % positions) / positions
                    real, imag = np.cos(angle), -np.sin(angle)
                    if f == 0:
                        real, imag = np.ones(length_first), (-1.0) ** a
                    first[col, at, target, 2 * f_at, j, :, j, :] = real.reshape(row_count, rows_first)
                    first[col, at, target, 2 * f_at + 1, j, :, j, :] = imag.reshape(row_count, rows_first)
    first = first.reshape(col_count, chunks, col_count * block * chunk, row_count, chunk * rows_first)
    rest = rows_second - (chunks - 1) * chunk
    last = first[:, -1, :, :, : rest * rows_first].reshape(col_count, col_count * block * chunk, -1)
    first = first.reshape(col_count, chunks, col_count * block * chunk, -1)
    first[:, -1] = 0.0
    first[:, -1, :, : last.shape[-1]] = last
    k_b = np.arange(length_second)
    second = np.zeros((2, 2, length_second, block, col_count, chunks, block, chunk))
    for other in range(2):
        for s in range(block):
            for source in range(col_count):
                for i in range(rows_second):
                    b = source * rows_second + i
                    f_at, upper = s % half, s >= half
                    at, j = divmod(i, chunk)
                    re_at, im_at = (source, at, 2 * f_at, j), (source, at, 2 * f_at + 1, j)
                    if other == 0 and f_at == 0:
                        shift = length_first // 2 if upper else 0
                        angle = 2 * np.pi * (b * (k_b * length_first + shift) % positions) / positions
                        place = im_at if upper else re_at
                        second[(other, 0, slice(None), s) + place] = np.cos(angle)
                        second[(other, 1, slice(None), s) + place] = np.sin(angle)
                        continue
                    sign = -1.0 if upper else 1.0
                    angle = 2 * np.pi * (b * (k_b + (1 if upper else 0)) % length_second) / length_second
                    second[(other, 0, slice(None), s) + re_at] = np.cos(angle)
                    second[(other, 0, slice(None), s) + im_at] = np.sin(angle) * sign
                    second[(other, 1, slice(None), s) + re_at] = np.sin(angle)
                    second[(other, 1, slice(None), s) + im_at] = -np.cos(angle) * sign
    second = second.reshape(2, 2, length_second * block, col_count * chunks * block * chunk)
    return first, second / math.sqrt(positions * GROUP)


def widened(packed, parts, used):
    count, rows, lanes = packed.shape
    flat = packed.reshape(count * rows, lanes).astype(jnp.float32)
    keep = lax.broadcasted_iota(jnp.int32, (1, lanes), 1) < used
    blocks = []
    for p in range(parts):
        block = flat if p == 0 else pltpu.roll(flat, lanes - p * used, 1)
        blocks.append(jnp.where(keep, block, 0.0).astype(packed.dtype).reshape(count, rows, lanes))
    return blocks


def packed_rows(values, parts, used):
    rows = values.shape[0] // parts
    total = values[:rows]
    for p in range(1, parts):
        total = total + pltpu.roll(values[p * rows : (p + 1) * rows], p * used, 1)
    return total


def kernel(
    n_r, n_c, parts, tokens, gain, w_in, forward, first, second, back, out,
    tok_v, norm_v, win_v, forward_v, first_v, second_v, back_v,
    sent1, came1, sent2, came2, sent3, came3, wide_v, wide3_v,
    load_sem, self_sem, send_sem1, recv_sem1, send_sem2, recv_sem2, send_sem3, recv_sem3,
):
    row, col = lax.axis_index("row"), lax.axis_index("col")
    rows, features = tokens.shape
    channels = w_in.shape[1]
    tiles = sent1.shape[0]
    span = n_r * GROUP
    spans = [(t * span, min(channels, (t + 1) * span)) for t in range(tiles)]
    width = GROUP // n_r
    used = (spans[-1][1] - spans[-1][0]) // GROUP * width
    order = [tiles - 1] + list(range(tiles - 1))

    barrier = pltpu.get_barrier_semaphore()
    for d in range(1, n_r):
        pl.semaphore_signal(barrier, inc=1, device_id={"row": lax.rem(row + d, n_r)}, device_id_type=MESH)
    for d in range(1, n_c):
        pl.semaphore_signal(barrier, inc=1, device_id={"col": lax.rem(col + d, n_c)}, device_id_type=MESH)

    load_tok = pltpu.make_async_copy(tokens, tok_v, load_sem.at[0])
    load_tok.start()
    load_win = [
        pltpu.make_async_copy(w_in.at[:, lo:hi], win_v.at[:, lo:hi], load_sem.at[6 + t])
        for t, (lo, hi) in enumerate(spans)
    ]
    load_forward = pltpu.make_async_copy(forward, forward_v, load_sem.at[1])
    load_first = pltpu.make_async_copy(first.at[col], first_v, load_sem.at[2])
    load_second = pltpu.make_async_copy(second.at[jnp.minimum(col, 1)], second_v, load_sem.at[3])
    load_back = pltpu.make_async_copy(back, back_v, load_sem.at[4])
    load_win[order[0]].start()
    load_forward.start()
    for t in order[1:]:
        load_win[t].start()
    load_first.start()
    load_second.start()

    load_tok.wait()
    floats = tok_v[...].astype(jnp.float32)
    inverse = lax.rsqrt(jnp.mean(floats * floats, axis=-1, keepdims=True) + norm_eps)
    gains = gain[...].astype(jnp.float32)
    for at in range(features // LANES):
        lanes = slice(at * LANES, (at + 1) * LANES)
        scaled = tok_v[:, lanes].astype(jnp.float32) * inverse * gains[at : at + 1, :]
        norm_v[:, lanes] = scaled.astype(jnp.bfloat16)

    def exchange(sent, came, send_sem, recv_sem, self_sem_at, t, me, count, axis):
        size = sent.shape[2]
        if axis == "row" and t == tiles - 1:
            size = size // parts
        own = pltpu.make_async_copy(sent.at[t, me, 0:size], came.at[t, me, 0:size], self_sem_at)
        copies = []
        for d in sorted(range(1, count), key=lambda d: -min(d, count - d)):
            target = lax.rem(me + d, count)
            copy = pltpu.make_async_remote_copy(
                src_ref=sent.at[t, target, 0:size],
                dst_ref=came.at[t, me, 0:size],
                send_sem=send_sem.at[t, d],
                recv_sem=recv_sem.at[t, d],
                device_id={axis: target},
                device_id_type=MESH,
            )
            copy.start()
            copies.append(copy)
        own.start()
        return [own] + copies

    steps1, steps2, steps3 = {}, {}, {}
    for t in order:
        lo, hi = spans[t]
        load_win[t].wait()
        mapped = jnp.dot(norm_v[...], win_v[:, lo:hi], preferred_element_type=jnp.float32).astype(jnp.bfloat16)
        if t == order[0]:
            load_forward.wait()
        for r in range(n_r):
            piece = jnp.dot(mapped, forward_v[r, : hi - lo, :], preferred_element_type=jnp.float32)
            if t == tiles - 1:
                sent1[t, r, 0 : rows // parts] = packed_rows(piece, parts, used).astype(jnp.bfloat16)
            else:
                sent1[t, r] = piece.astype(jnp.bfloat16)
        if t == order[0]:
            pl.semaphore_wait(barrier, n_r + n_c - 2)
        steps1[t] = exchange(sent1, came1, send_sem1, recv_sem1, self_sem.at[0, t], t, row, n_r, "row")

    load_back.start()
    load_first.wait()
    chunks, high, depth = first_v.shape
    step = depth // n_r
    height = high // n_c
    for t in order:
        for copy in steps1[t]:
            copy.wait()
        source = came1.at[t]
        if t == tiles - 1:
            size = rows // parts
            for p, block in enumerate(widened(came1[t, :, 0:size], parts, used)):
                wide_v[:, p * size : (p + 1) * size] = block
            source = wide_v
        for at in range(chunks):
            values = source[:, at * step : min(rows, (at + 1) * step)]
            values = values.reshape(-1, LANES)
            turned = jnp.dot(first_v[at, :, : values.shape[0]], values, preferred_element_type=jnp.float32)
            turned = turned.astype(jnp.bfloat16).reshape(n_c, height, LANES)
            sent2[t, :, at * height : (at + 1) * height] = turned
        steps2[t] = exchange(sent2, came2, send_sem2, recv_sem2, self_sem.at[1, t], t, col, n_c, "col")

    lane = lax.broadcasted_iota(jnp.int32, (1, LANES), 1) % width
    cosine = (lane < width // 2) | ((lane == width // 2) & (row == 0))
    load_second.wait()
    out_rows = sent3.shape[2]
    for t in order:
        for copy in steps2[t]:
            copy.wait()
        values = came2[t].reshape(-1, LANES)
        even = jnp.dot(second_v[0], values, preferred_element_type=jnp.float32)
        odd = jnp.dot(second_v[1], values, preferred_element_type=jnp.float32)
        both = jnp.where(cosine, even, odd)
        if t == tiles - 1:
            for r in range(n_r):
                block = packed_rows(both[r * out_rows : (r + 1) * out_rows], parts, used)
                sent3[t, r, 0 : out_rows // parts] = block.astype(jnp.bfloat16)
        else:
            sent3[t] = both.astype(jnp.bfloat16).reshape(sent3.shape[1:])
        steps3[t] = exchange(sent3, came3, send_sem3, recv_sem3, self_sem.at[2, t], t, row, n_r, "row")

    load_back.wait()
    for t in order:
        lo, hi = spans[t]
        for copy in steps3[t]:
            copy.wait()
        source = came3.at[t]
        if t == tiles - 1:
            size = out_rows // parts
            for p, block in enumerate(widened(came3[t, :, 0:size], parts, used)):
                wide3_v[:, p * size : (p + 1) * size] = block
            source = wide3_v
        total = jnp.dot(source[0], back_v[0, :, : hi - lo], preferred_element_type=jnp.float32)
        for r in range(1, n_r):
            total = total + jnp.dot(source[r], back_v[r, :, : hi - lo], preferred_element_type=jnp.float32)
        out[:, lo:hi] = total.astype(jnp.bfloat16)


def last_product(spectrum, w_out, out):
    total = jnp.dot(spectrum[...], w_out[...], preferred_element_type=jnp.float32)
    out[...] = total.reshape(out.shape).astype(jnp.bfloat16)


def fused_shards(n_r, n_c, tokens, norm_gain, w_in, w_out):
    rows_first, rows_second, features = tokens.shape
    channels = w_in.shape[1]
    length_first = rows_first * n_r
    block = length_first // n_c
    chunk = SUBLANES // block
    chunks = -(-rows_second // chunk)
    padded = chunks * SUBLANES
    groups = channels // GROUP
    tiles = -(-groups // n_r)
    rows = rows_first * rows_second
    length_second = rows_second * n_c
    out_rows = length_second // n_r * block
    forward, back = channel_tables(n_r)
    first, second = position_tables(rows_first, rows_second, n_r, n_c, chunk, chunks)
    used = (groups - (tiles - 1) * n_r) * (GROUP // n_r)
    parts = max(p for p in range(1, LANES // used + 1) if rows % (SUBLANES * p) == 0 and out_rows % (SUBLANES * p) == 0)
    tokens = tokens.transpose(1, 0, 2).reshape(rows, features)
    kind = jnp.bfloat16
    tables = [jnp.asarray(np.asarray(x, np.float32).astype(kind)) for x in (forward, first, second, back)]
    anywhere = pl.BlockSpec(memory_space=pl.ANY)
    vmem = pl.BlockSpec(memory_space=pltpu.VMEM)
    dma = pltpu.SemaphoreType.DMA
    spectrum = pl.pallas_call(
        functools.partial(kernel, n_r, n_c, parts),
        out_shape=jax.ShapeDtypeStruct((out_rows, channels), kind),
        in_specs=[anywhere, vmem] + [anywhere] * 5,
        out_specs=vmem,
        scratch_shapes=[
            pltpu.VMEM(tokens.shape, kind),
            pltpu.VMEM((rows, features), kind),
            pltpu.VMEM(w_in.shape, kind),
            pltpu.VMEM(forward.shape, kind),
            pltpu.VMEM(first.shape[1:], kind),
            pltpu.VMEM(second.shape[1:], kind),
            pltpu.VMEM(back.shape, kind),
            pltpu.VMEM((tiles, n_r, rows, LANES), kind),
            pltpu.VMEM((tiles, n_r, rows, LANES), kind),
            pltpu.VMEM((tiles, n_c, padded, LANES), kind),
            pltpu.VMEM((tiles, n_c, padded, LANES), kind),
            pltpu.VMEM((tiles, n_r, out_rows, LANES), kind),
            pltpu.VMEM((tiles, n_r, out_rows, LANES), kind),
            pltpu.VMEM((n_r, rows, LANES), kind),
            pltpu.VMEM((n_r, out_rows, LANES), kind),
            dma((6 + tiles,)),
            dma((3, tiles)),
            dma((tiles, n_r)),
            dma((tiles, n_r)),
            dma((tiles, n_c)),
            dma((tiles, n_c)),
            dma((tiles, n_r)),
            dma((tiles, n_r)),
        ],
        compiler_params=pltpu.CompilerParams(
            collective_id=0, has_side_effects=True, vmem_limit_bytes=53 * 1024 * 1024
        ),
    )(tokens, norm_gain.reshape(-1, LANES), w_in, *tables)
    return pl.pallas_call(
        last_product,
        out_shape=jax.ShapeDtypeStruct((length_second // n_r, block, features), kind),
        in_specs=[vmem] * 2,
        out_specs=vmem,
        compiler_params=pltpu.CompilerParams(vmem_limit_bytes=16 * 1024 * 1024),
    )(spectrum, w_out)


def fits(n_r, n_c, tokens_shape, channels):
    length_first, length_second, _ = tokens_shape
    rows = length_first // n_r * (length_second // n_c)
    out_rows = length_second // n_r * (length_first // n_c)
    return (
        GROUP % (2 * n_r) == 0
        and length_first % (2 * n_c) == 0
        and SUBLANES % (length_first // n_c) == 0
        and rows % SUBLANES == 0
        and out_rows % SUBLANES == 0
        and length_first // n_r * (SUBLANES // (length_first // n_c)) % SUBLANES == 0
        and length_second % n_r == 0
    )


def tables(length):
    series = jnp.arange(length, dtype=jnp.int32)
    product = series[:, None] * series[None, :] % length
    angles = product.astype(jnp.float32) * (2.0 * math.pi / length)
    return (jnp.cos(angles), jnp.sin(angles))


def folded_order(length_first, devices):
    block = length_first // devices
    half_block = block // 2
    series = jnp.arange(length_first, dtype=jnp.int32)
    device = series // block
    inner = series % block
    lower = device * half_block + inner
    upper = length_first - device * half_block - (inner - half_block)
    upper = jnp.where((device == 0) & (inner == half_block), length_first // 2, upper)
    return jnp.where(inner < half_block, lower, upper) % length_first


def to_channels(values, row_count):
    rows_first, rows_second, channels = values.shape
    width = channels // row_count
    parted = values.reshape(rows_first, rows_second, row_count, width).transpose(2, 0, 1, 3)
    return parted.reshape(row_count * rows_first, rows_second * width)


def product(table, values):
    return jnp.dot(table, values, precision=highest)


def middle(real_part, imag_part, width):
    length_first = real_part.shape[0]
    rows_second = real_part.shape[1] // width
    col_count = lax.axis_size("col")
    length_second = rows_second * col_count
    positions = length_first * length_second
    frequency = folded_order(length_first, col_count)
    series = jnp.arange(length_first, dtype=jnp.int32)
    first_angle = (frequency[:, None] * series[None, :] % length_first).astype(jnp.float32)
    first_angle = first_angle * (2.0 * math.pi / length_first)
    first_cos = jnp.cos(first_angle)
    first_sin = jnp.sin(first_angle)
    first_real = product(first_cos, real_part)
    first_imag = -product(first_sin, real_part)
    first_real = first_real + product(first_sin, imag_part)
    first_imag = first_imag + product(first_cos, imag_part)
    first_real = first_real.reshape(length_first, rows_second, width)
    first_imag = first_imag.reshape(length_first, rows_second, width)
    second_index = lax.axis_index("col") * rows_second + jnp.arange(rows_second, dtype=jnp.int32)
    twiddle_angle = (frequency[:, None] * second_index[None, :] % positions).astype(jnp.float32)
    twiddle_angle = twiddle_angle * (2.0 * math.pi / positions)
    twiddle_cos = jnp.cos(twiddle_angle)[:, :, None]
    twiddle_sin = jnp.sin(twiddle_angle)[:, :, None]
    turned_real = first_real * twiddle_cos + first_imag * twiddle_sin
    turned_imag = first_imag * twiddle_cos - first_real * twiddle_sin
    turned = jnp.stack([turned_real, turned_imag]).transpose(0, 2, 1, 3)
    turned = turned.reshape(2, rows_second, length_first * width)
    exchanged = lax.all_to_all(
        turned.astype(jnp.bfloat16), "col", split_axis=2, concat_axis=1, tiled=True
    ).astype(turned.dtype)
    second_cos, second_sin = tables(length_second)
    block = length_first // col_count
    out_shape = (length_second, block, width)
    out_real = (product(second_cos, exchanged[0]) + product(second_sin, exchanged[1])).reshape(
        out_shape
    )
    return out_real


def shards(tokens, norm_gain, w_in, w_out):
    rows_first, rows_second, features = tokens.shape
    row_count = lax.axis_size("row")
    length_first = rows_first * row_count
    length_second = rows_second * lax.axis_size("col")
    channels = w_in.shape[1]
    width = channels // row_count
    groups = channels // GROUP
    scaling = 1.0 / math.sqrt(length_first * length_second * GROUP)
    floats = tokens.astype(jnp.float32)
    normed = (
        floats
        * lax.rsqrt(jnp.mean(floats * floats, axis=-1, keepdims=True) + norm_eps)
        * norm_gain.astype(jnp.float32)
    ).astype(jnp.bfloat16)
    mapped = jnp.dot(normed.reshape(-1, features), w_in, preferred_element_type=jnp.float32)
    mapped = mapped.astype(jnp.bfloat16).reshape(rows_first, rows_second, channels)
    channel_cos, channel_sin = tables(GROUP)
    grouped = mapped.astype(jnp.float32).reshape(rows_first, rows_second, groups, GROUP)
    spec_real = jnp.einsum("abgj,jm->abgm", grouped, channel_cos, precision=highest)
    spec_imag = -jnp.einsum("abgj,jm->abgm", grouped, channel_sin, precision=highest)
    stacked = jnp.stack(
        [
            to_channels(spec_real.reshape(rows_first, rows_second, channels), row_count),
            to_channels(spec_imag.reshape(rows_first, rows_second, channels), row_count),
        ]
    )
    arrived = lax.all_to_all(
        stacked.astype(jnp.bfloat16), "row", split_axis=1, concat_axis=1, tiled=True
    ).astype(stacked.dtype)
    result = middle(arrived[0], arrived[1], width)
    spectrum = (result * scaling).astype(jnp.bfloat16)
    returned = lax.all_to_all(spectrum, "row", split_axis=0, concat_axis=2, tiled=True)
    mixed = jnp.dot(returned.reshape(-1, channels), w_out, preferred_element_type=jnp.float32)
    return mixed.astype(jnp.bfloat16).reshape(returned.shape[0], returned.shape[1], features)


def solution(mesh):
    in_specs = (P("row", "col", None), P(), P(), P())
    out_specs = P("row", "col", None)
    n_r, n_c = mesh.shape["row"], mesh.shape["col"]

    def run(tokens, norm_gain, w_in, w_out):
        whole = fits(n_r, n_c, tokens.shape, w_in.shape[1])
        body = functools.partial(fused_shards, n_r, n_c) if whole else shards
        return jax.shard_map(body, mesh=mesh, in_specs=in_specs, out_specs=out_specs, check_vma=False)(
            tokens, norm_gain, w_in, w_out
        )

    return run
```

profile of v0, /device:TPU:0, one launch (start us, length us, event | category | flops | bytes accessed | tf_op | source)
XLA Modules:
  0.0 30.7 jit_solution(10925504428118059262)
XLA Ops:
  0.0 0.0 copy-start.1
  0.0 1.0 %copy-done.1 = bf16[4,512,128]{2,1,0:T(8,128)(2,1)S(1)} copy-done((bf16[4,512,128]{2,1,0:T(8,128)(2,1)S(1)}, bf16[4,512,128]{2,1,0:T(8,128)(2,1)}, u32[]{:S(2)}) %copy-start.1) | copy-done | bytes 524312
  1.0 0.0 copy-start.2
  1.0 0.7 %copy-done.2 = bf16[2048]{0:T(1024)(128)(2,1)S(1)} copy-done((bf16[2048]{0:T(1024)(128)(2,1)S(1)}, bf16[2048]{0:T(1024)(128)(2,1)}, u32[]{:S(2)}) %copy-start.2) | copy-done | bytes 4120
  1.7 0.0 copy-start
  1.7 27.1 %shard_map.82.spectrum = bf16[144,1152]{1,0:T(8,128)(2,1)S(1)} custom-call(bf16[144,2048]{1,0:T(8,128)(2,1)} %bitcast.5, bf16[16,128]{1,0:T(8,128)(2,1)S(1)} %bitcast.4, bf16[2048,1152]{1,0:T(8,128)(2,1)} %w_in.1, bf16[4,512,128]{2,1,0:T(8,128)(2,1)S(1)} %copy-done.1, bf16[8,5,128,128]{3,2,1,0:T(8,128)(2,1)} %constant.9.clone.first, ...), custom_call_target="tpu_custom_call" | custom-call | tf_op jit(solution)/shard_map/pallas_call | solution.py:308
  28.8 0.0 copy-done
  28.8 1.9 %shard_map.83 = bf16[36,4,2048]{2,1,0:T(4,128)(2,1)} custom-call(bf16[144,1152]{1,0:T(8,128)(2,1)S(1)} %shard_map.82.spectrum, bf16[1152,2048]{1,0:T(8,128)(2,1)S(1)} %copy-done), custom_call_target="tpu_custom_call" | custom-call | tf_op jit(solution)/shard_map/pallas_call | solution.py:342
Async XLA Ops:
  0.0 1.0 %copy-start.1 = (bf16[4,512,128]{2,1,0:T(8,128)(2,1)S(1)}, bf16[4,512,128]{2,1,0:T(8,128)(2,1)}, u32[]{:S(2)}) copy-start(bf16[4,512,128]{2,1,0:T(8,128)(2,1)} %constant.8.clone.forward) | copy-start | bytes 1572868
  1.0 0.7 %copy-start.2 = (bf16[2048]{0:T(1024)(128)(2,1)S(1)}, bf16[2048]{0:T(1024)(128)(2,1)}, u32[]{:S(2)}) copy-start(bf16[2048]{0:T(1024)(128)(2,1)} %param.9) | copy-start | bytes 12292
  1.7 27.1 %copy-start = (bf16[1152,2048]{1,0:T(8,128)(2,1)S(1)}, bf16[1152,2048]{1,0:T(8,128)(2,1)}, u32[]{:S(2)}) copy-start(bf16[1152,2048]{1,0:T(8,128)(2,1)} %w_out.1) | copy-start | bytes 14155780
where the time goes:
time: 30.9 us; the launch traced here: 30.7 us
  Pallas kernels  28.9 us (94%)
  local copies, waits for them, and re-layouts  1.73 us (6%)
    pallas_call x1, Pallas kernels, fused_shards(): pl.pallas_call(functools.partial(kernel, n_r, n_c, parts), out_shape=jax....  27.1 us
    pallas_call x1, Pallas kernels, fused_shards(): pl.pallas_call(last_product, out_shape=jax.ShapeDtypeStruct((length_secon...  1.86 us
    unnamed x6, local copies, waits for them, and re-layouts  1.73 us

commit v1 on v0

--- a/solution.py
+++ b/solution.py
@@ -135,7 +135,7 @@
 
 def kernel(
     n_r, n_c, parts, tokens, gain, w_in, forward, first, second, back, out,
-    tok_v, norm_v, win_v, forward_v, first_v, second_v, back_v,
+    tok_v, gain_v, norm_v, win_v, forward_v, first_v, second_v, back_v,
     sent1, came1, sent2, came2, sent3, came3, wide_v, wide3_v,
     load_sem, self_sem, send_sem1, recv_sem1, send_sem2, recv_sem2, send_sem3, recv_sem3,
 ):
@@ -157,6 +157,8 @@
 
     load_tok = pltpu.make_async_copy(tokens, tok_v, load_sem.at[0])
     load_tok.start()
+    load_gain = pltpu.make_async_copy(gain, gain_v, load_sem.at[5])
+    load_gain.start()
     load_win = [
         pltpu.make_async_copy(w_in.at[:, lo:hi], win_v.at[:, lo:hi], load_sem.at[6 + t])
         for t, (lo, hi) in enumerate(spans)
@@ -173,9 +175,10 @@
     load_second.start()
 
     load_tok.wait()
+    load_gain.wait()
     floats = tok_v[...].astype(jnp.float32)
     inverse = lax.rsqrt(jnp.mean(floats * floats, axis=-1, keepdims=True) + norm_eps)
-    gains = gain[...].astype(jnp.float32)
+    gains = gain_v[...].astype(jnp.float32)
     for at in range(features // LANES):
         lanes = slice(at * LANES, (at + 1) * LANES)
         scaled = tok_v[:, lanes].astype(jnp.float32) * inverse * gains[at : at + 1, :]
@@ -302,16 +305,17 @@
     tokens = tokens.transpose(1, 0, 2).reshape(rows, features)
     kind = jnp.bfloat16
     tables = [jnp.asarray(np.asarray(x, np.float32).astype(kind)) for x in (forward, first, second, back)]
-    anywhere = pl.BlockSpec(memory_space=pl.ANY)
+    hbm = pl.BlockSpec(memory_space=pltpu.HBM)
     vmem = pl.BlockSpec(memory_space=pltpu.VMEM)
     dma = pltpu.SemaphoreType.DMA
     spectrum = pl.pallas_call(
         functools.partial(kernel, n_r, n_c, parts),
-        out_shape=jax.ShapeDtypeStruct((out_rows, channels), kind),
-        in_specs=[anywhere, vmem] + [anywhere] * 5,
+        out_shape=pltpu.VMEM((out_rows, channels), kind),
+        in_specs=[hbm] * 7,
         out_specs=vmem,
         scratch_shapes=[
             pltpu.VMEM(tokens.shape, kind),
+            pltpu.VMEM((features // LANES, LANES), kind),
             pltpu.VMEM((rows, features), kind),
             pltpu.VMEM(w_in.shape, kind),
             pltpu.VMEM(forward.shape, kind),
@@ -338,7 +342,7 @@
         compiler_params=pltpu.CompilerParams(
             collective_id=0, has_side_effects=True, vmem_limit_bytes=53 * 1024 * 1024
         ),
-    )(tokens, norm_gain.reshape(-1, LANES), w_in, *tables)
+    )(*[pltpu.with_memory_space_constraint(x, pltpu.HBM) for x in (tokens, norm_gain.reshape(-1, LANES), w_in, *tables)])
     return pl.pallas_call(
         last_product,
         out_shape=jax.ShapeDtypeStruct((length_second // n_r, block, features), kind),

time: 30.9 us -> 28.9 us (0.935)
  local copies, waits for them, and re-layouts: 1.73 us -> 0.01 us
    unnamed x6 -> x2, local copies, waits for them, and re-layouts: 1.73 us -> 0.01 us
where the time goes in v1:
time: 28.9 us; the launch traced here: 28.7 us
  Pallas kernels  28.7 us (99%)
    pallas_call x1, Pallas kernels, fused_shards(): pl.pallas_call(functools.partial(kernel, n_r, n_c, parts), out_shape=pltp...  26.9 us
    pallas_call x1, Pallas kernels, fused_shards(): pl.pallas_call(last_product, out_shape=jax.ShapeDtypeStruct((length_secon...  1.86 us

profile of v1, /device:TPU:0, one launch (start us, length us, event | category | flops | bytes accessed | tf_op | source)
XLA Modules:
  0.0 28.7 jit_solution(17063390742870057500)
XLA Ops:
  0.0 0.0 copy-start
  0.0 26.9 %shard_map.82.spectrum = bf16[144,1152]{1,0:T(8,128)(2,1)S(1)} custom-call(bf16[144,2048]{1,0:T(8,128)(2,1)} %bitcast.4, bf16[16,128]{1,0:T(8,128)(2,1)} %bitcast.5, bf16[2048,1152]{1,0:T(8,128)(2,1)} %w_in.1, bf16[4,512,128]{2,1,0:T(8,128)(2,1)} %constant.8.clone.forward, bf16[8,5,128,128]{3,2,1,0:T(8,128)(2,1)} %constant.9.clone.first, ...), custom_call_target="tpu_custom_call" | custom-call | tf_op jit(solution)/shard_map/pallas_call | solution.py:311
  26.9 0.0 copy-done
  26.9 1.9 %shard_map.83 = bf16[36,4,2048]{2,1,0:T(4,128)(2,1)} custom-call(bf16[144,1152]{1,0:T(8,128)(2,1)S(1)} %shard_map.82.spectrum, bf16[1152,2048]{1,0:T(8,128)(2,1)S(1)} %copy-done), custom_call_target="tpu_custom_call" | custom-call | tf_op jit(solution)/shard_map/pallas_call | solution.py:346
Async XLA Ops:
  0.0 26.9 %copy-start = (bf16[1152,2048]{1,0:T(8,128)(2,1)S(1)}, bf16[1152,2048]{1,0:T(8,128)(2,1)}, u32[]{:S(2)}) copy-start(bf16[1152,2048]{1,0:T(8,128)(2,1)} %w_out.1) | copy-start | bytes 14155780

commit v2 on v1

v2 whole, which is shorter than its diff:
```python
import functools
import math

import jax
import jax.numpy as jnp
import numpy as np
from jax import lax
from jax.experimental import pallas as pl
from jax.experimental.pallas import tpu as pltpu
from jax.sharding import PartitionSpec as P

GROUP = 128
LANES = 128
SUBLANES = 16
ROWS = 8
LAG = 2
MESH = pl.DeviceIdType.MESH


norm_eps = 1e-06
highest = lax.Precision.HIGHEST


def folded_list(length_first, devices):
    block = length_first // devices
    half = block // 2
    result = np.zeros(length_first, np.int64)
    for device in range(devices):
        for inner in range(block):
            if inner < half:
                value = device * half + inner
            elif device == 0 and inner == half:
                value = length_first // 2
            else:
                value = length_first - device * half - (inner - half)
            result[device * block + inner] = value % length_first
    return result


def ceil_to(value, multiple):
    return -(-value // multiple) * multiple


class Piece:
    def __init__(self, groups, n_r, n_c, rows_first, rows_second, length_second):
        self.groups = groups
        self.channels = groups * GROUP
        self.used = groups * GROUP // n_r
        self.parts = LANES // self.used
        self.seconds = -(-rows_second // self.parts)
        self.block = rows_first * n_r // n_c
        self.rows1 = self.seconds * rows_first
        self.rows2 = ceil_to(self.seconds * self.block, ROWS)
        self.out_rows = length_second // n_r * self.block
        self.rows3 = ceil_to(-(-self.out_rows // self.parts), ROWS)


def chunk_sizes(groups, n_r):
    per = LANES // 2 // (GROUP // n_r)
    rest = groups % per
    return [per] * (groups // per) + ([rest] if rest else [])


def channel_tables(piece, n_r):
    width = GROUP // n_r
    half = width // 2
    j = np.arange(GROUP)
    forward = np.zeros((piece.parts, piece.groups, GROUP, n_r, piece.parts, piece.groups, width))
    back = np.zeros((n_r, piece.parts, piece.groups, width, piece.parts, piece.groups, GROUP))
    for row in range(n_r):
        for x in range(width):
            m = row * half + x % half
            cosine = x < half
            column = np.cos(2 * np.pi * j * m / GROUP) if cosine else np.sin(2 * np.pi * j * m / GROUP)
            entries = [(m, 1.0)]
            if not cosine and m == 0:
                column = np.cos(np.pi * j)
                entries = [(GROUP // 2, 1.0)]
            elif m:
                entries = [(m, 1.0 if cosine else -1.0), (GROUP - m, 1.0)]
            for q in range(piece.parts):
                for g in range(piece.groups):
                    forward[q, g, :, row, q, g, x] = column
                    for at, sign in entries:
                        back[row, q, g, x, q, g, at] = sign
    size = piece.parts * piece.channels
    return forward.reshape(size, n_r * LANES), back.reshape(n_r * LANES, size)


def position_tables(piece, rows_first, rows_second, n_r, n_c):
    length_first = rows_first * n_r
    length_second = rows_second * n_c
    positions = length_first * length_second
    block, parts, seconds = piece.block, piece.parts, piece.seconds
    half = block // 2
    a = np.arange(length_first)
    first = np.zeros((n_c, parts, n_c, piece.rows2, n_r, seconds, rows_first))
    for col in range(n_c):
        for i in range(rows_second):
            q, j = divmod(i, seconds)
            p = a * length_second + col * rows_second + i
            for target in range(n_c):
                for f_at in range(half):
                    f = target * half + f_at
                    angle = 2 * np.pi * (f * p % positions) / positions
                    real, imag = np.cos(angle), -np.sin(angle)
                    if f == 0:
                        real, imag = np.ones(length_first), (-1.0) ** a
                    first[col, q, target, j * block + 2 * f_at, :, j, :] = real.reshape(n_r, rows_first)
                    first[col, q, target, j * block + 2 * f_at + 1, :, j, :] = imag.reshape(n_r, rows_first)
    k_b = np.arange(length_second)
    plain = np.zeros((2, 2, length_second, block, parts, n_c, piece.rows2))
    for other in range(2):
        for s in range(block):
            for source in range(n_c):
                for i in range(rows_second):
                    b = source * rows_second + i
                    f_at, upper = s % half, s >= half
                    q, j = divmod(i, seconds)
                    re_at, im_at = (q, source, j * block + 2 * f_at), (q, source, j * block + 2 * f_at + 1)
                    if other == 0 and f_at == 0:
                        shift = length_first // 2 if upper else 0
                        angle = 2 * np.pi * (b * (k_b * length_first + shift) % positions) / positions
                        place = im_at if upper else re_at
                        plain[(other, 0, slice(None), s) + place] = np.cos(angle)
                        plain[(other, 1, slice(None), s) + place] = np.sin(angle)
                        continue
                    sign = -1.0 if upper else 1.0
                    angle = 2 * np.pi * (b * (k_b + (1 if upper else 0)) % length_second) / length_second
                    plain[(other, 0, slice(None), s) + re_at] = np.cos(angle)
                    plain[(other, 0, slice(None), s) + im_at] = np.sin(angle) * sign
                    plain[(other, 1, slice(None), s) + re_at] = np.sin(angle)
                    plain[(other, 1, slice(None), s) + im_at] = -np.cos(angle) * sign
    plain = plain.reshape(2, 2, n_r, piece.out_rows, parts, n_c * piece.rows2) / math.sqrt(positions * GROUP)
    second = np.zeros((2, n_r, parts, 2, piece.rows3, parts, n_c * piece.rows2))
    for q in range(parts):
        lo, hi = q * piece.rows3, min(piece.out_rows, (q + 1) * piece.rows3)
        for d in range(parts):
            values = plain[:, :, :, lo:hi, (q - d) % parts]
            second[:, :, q, :, : hi - lo, d] = values.transpose(0, 2, 1, 3, 4)
    first = first.reshape(n_c, parts * n_c * piece.rows2, n_r * piece.rows1)
    return first, second.reshape(2, n_r, parts * 2 * piece.rows3, parts * n_c * piece.rows2)


def bits_apart(one, other, count):
    total, bit = 0, 1
    while bit < count:
        total = total + bit * ((one // bit + other // bit) % 2)
        bit *= 2
    return total


def far_first(me, count):
    places = []
    for k in range(count - 1):
        down = count - 1 - k - jnp.where(count - 1 - k <= me, 1, 0)
        up = k + jnp.where(k >= me, 1, 0)
        places.append(jnp.where(me < count // 2, down, up))
    return places


def kernel(n_r, n_c, pieces, kinds, *refs):
    refs = list(refs)

    def take(count):
        taken = refs[:count]
        del refs[:count]
        return taken

    many = len(pieces)
    tokens, gain, w_in = take(3)
    tables_hbm = [take(4) for _ in pieces]
    (out,) = take(1)
    tok_v, gain_v, norm_v, win_v = take(4)
    tables_v = [take(4) for _ in pieces]
    buffers = [take(6) for _ in pieces]
    load_sem, table_sem, self_sem, send1, recv1, send2, recv2, send3, recv3 = take(9)
    row, col = lax.axis_index("row"), lax.axis_index("col")
    rows, features = tokens.shape
    steps = len(kinds)
    spans, seats = [], []
    lo = 0
    for at, kind in enumerate(kinds):
        spans.append((lo, lo + pieces[kind].channels))
        seats.append(kinds[:at].count(kind))
        lo = spans[-1][1]

    barrier = pltpu.get_barrier_semaphore()
    for d in range(1, n_r):
        pl.semaphore_signal(barrier, inc=1, device_id={"row": bits_apart(row, d, n_r)}, device_id_type=MESH)
    for d in range(1, n_c):
        pl.semaphore_signal(barrier, inc=1, device_id={"col": bits_apart(col, d, n_c)}, device_id_type=MESH)

    load_tok = pltpu.make_async_copy(tokens, tok_v, load_sem.at[0])
    load_gain = pltpu.make_async_copy(gain, gain_v, load_sem.at[1])
    load_win = [
        pltpu.make_async_copy(w_in.at[:, lo:hi], win_v.at[:, lo:hi], load_sem.at[2 + t])
        for t, (lo, hi) in enumerate(spans)
    ]
    load = []
    for p, (forward, first, second, back) in enumerate(tables_hbm):
        sources = (forward, first.at[col], second.at[jnp.minimum(col, 1)], back)
        load.append(
            [pltpu.make_async_copy(x, y, table_sem.at[p, n]) for n, (x, y) in enumerate(zip(sources, tables_v[p]))]
        )
    load_tok.start()
    load_gain.start()
    started = set()
    for t, kind in enumerate(kinds):
        load_win[t].start()
        if kind not in started:
            load[kind][0].start()
            started.add(kind)
    for n in (1, 2):
        for p in range(many):
            load[p][n].start()
    pending = {(p, n) for p in range(many) for n in range(4)}

    def table(p, n):
        if (p, n) in pending:
            load[p][n].wait()
            pending.discard((p, n))
        return tables_v[p][n]

    load_tok.wait()
    load_gain.wait()
    floats = tok_v[...].astype(jnp.float32)
    inverse = lax.rsqrt(jnp.mean(floats * floats, axis=-1, keepdims=True) + norm_eps)
    gains = gain_v[...].astype(jnp.float32)
    for at in range(features // LANES):
        lanes = slice(at * LANES, (at + 1) * LANES)
        scaled = tok_v[:, lanes].astype(jnp.float32) * inverse * gains[at : at + 1, :]
        norm_v[:, lanes] = scaled.astype(jnp.bfloat16)

    row_targets = far_first(row, n_r)
    col_targets = [bits_apart(col, d, n_c) for d in range(n_c - 1, 0, -1)]
    stages = (
        (row, row_targets, send1, recv1, "row"),
        (col, col_targets, send2, recv2, "col"),
        (row, row_targets, send3, recv3, "row"),
    )

    def send(sent, came, stage, seat, t, target):
        me, targets, send_sem, recv_sem, axis = stages[stage]
        d = bits_apart(me, target, len(targets) + 1)
        copy = pltpu.make_async_remote_copy(
            src_ref=sent.at[seat, target],
            dst_ref=came.at[seat, me],
            send_sem=send_sem.at[t, d],
            recv_sem=recv_sem.at[t, d],
            device_id={axis: target},
            device_id_type=MESH,
        )
        copy.start()
        return copy

    def keep(sent, came, stage, seat, t):
        me = stages[stage][0]
        copy = pltpu.make_async_copy(sent.at[seat, me], came.at[seat, me], self_sem.at[stage, t])
        copy.start()
        return copy

    def exchange(sent, came, stage, seat, t):
        copies = [send(sent, came, stage, seat, t, target) for target in stages[stage][1]]
        return copies + [keep(sent, came, stage, seat, t)]

    lane = lax.broadcasted_iota(jnp.int32, (1, LANES), 1)
    turn = lane % (GROUP // n_r)
    cosine = (turn < GROUP // n_r // 2) | ((turn == GROUP // n_r // 2) & (row == 0))
    copies1, copies2, copies3 = {}, {}, {}

    def start(t):
        p, seat = kinds[t], seats[t]
        piece = pieces[p]
        lo, hi = spans[t]
        load_win[t].wait()
        mapped = jnp.dot(norm_v[...], win_v[:, lo:hi], preferred_element_type=jnp.float32)
        short = piece.parts * piece.rows1 - rows
        if short:
            mapped = jnp.concatenate([mapped, jnp.zeros((short, hi - lo), jnp.float32)], axis=0)
        blocks = [mapped[q * piece.rows1 : (q + 1) * piece.rows1] for q in range(piece.parts)]
        side = jnp.concatenate(blocks, axis=1).astype(jnp.bfloat16)
        turned = jnp.dot(side, table(p, 0)[...], preferred_element_type=jnp.float32).astype(jnp.bfloat16)
        sent, came = buffers[p][:2]
        for r in range(n_r):
            sent[seat, r] = turned[:, r * LANES : (r + 1) * LANES]
        if t == 0:
            pl.semaphore_wait(barrier, n_r + n_c - 2)
        copies1[t] = exchange(sent, came, 0, seat, t)

    def middle_first(t):
        p, seat = kinds[t], seats[t]
        piece = pieces[p]
        weights = table(p, 1)
        for copy in copies1[t]:
            copy.wait()
        values = buffers[p][1][seat].reshape(n_r * piece.rows1, LANES)
        both = jnp.dot(weights[...], values, preferred_element_type=jnp.float32)
        size = n_c * piece.rows2
        total = both[:size]
        for q in range(1, piece.parts):
            total = jnp.where(lane < q * piece.used, total, both[q * size : (q + 1) * size])
        sent, came = buffers[p][2:4]
        sent[seat] = total.astype(jnp.bfloat16).reshape(n_c, piece.rows2, LANES)
        copies2[t] = exchange(sent, came, 1, seat, t)

    def middle_second(t):
        p, seat = kinds[t], seats[t]
        piece = pieces[p]
        weights = table(p, 2)
        for copy in copies2[t]:
            copy.wait()
        values = buffers[p][3][seat].reshape(n_c * piece.rows2, LANES)
        floats = values.astype(jnp.float32)
        rolled = [values] + [
            pltpu.roll(floats, d * piece.used, 1).astype(jnp.bfloat16) for d in range(1, piece.parts)
        ]
        deep = jnp.concatenate(rolled, axis=0)
        sent, came = buffers[p][4:6]
        size = piece.rows3
        for r in range(n_r):
            both = jnp.dot(weights[r], deep, preferred_element_type=jnp.float32)
            chosen = [
                jnp.where(cosine, both[2 * q * size : (2 * q + 1) * size], both[(2 * q + 1) * size : (2 * q + 2) * size])
                for q in range(piece.parts)
            ]
            total = chosen[0]
            for q in range(1, piece.parts):
                total = jnp.where(lane < q * piece.used, total, chosen[q])
            sent[seat, r] = total.astype(jnp.bfloat16)
        copies3[t] = exchange(sent, came, 2, seat, t)

    def finish(t):
        p, seat = kinds[t], seats[t]
        piece = pieces[p]
        lo, hi = spans[t]
        weights = table(p, 3)
        for copy in copies3[t]:
            copy.wait()
        side = jnp.concatenate([buffers[p][5][seat, r] for r in range(n_r)], axis=1)
        total = jnp.dot(side, weights[...], preferred_element_type=jnp.float32).astype(jnp.bfloat16)
        size = piece.channels
        for q in range(piece.parts):
            above, below = q * piece.rows3, min(piece.out_rows, (q + 1) * piece.rows3)
            out[above:below, lo:hi] = total[: below - above, q * size : (q + 1) * size]

    for t in range(steps):
        start(t)
    for p in range(many):
        load[p][3].start()
    for job, t in schedule(steps):
        (middle_first, middle_second, finish)[job](t)


def schedule(steps):
    jobs, ready = [], 0
    for t in range(steps):
        jobs.append((0, t))
        while ready <= t - LAG:
            jobs.append((1, ready))
            ready += 1
    jobs += [(1, t) for t in range(ready, steps)]
    return jobs + [(2, t) for t in range(steps)]


def last_product(spectrum, w_out, out):
    total = jnp.dot(spectrum[...], w_out[...], preferred_element_type=jnp.float32)
    out[...] = total.reshape(out.shape).astype(jnp.bfloat16)


def fused_shards(n_r, n_c, tokens, norm_gain, w_in, w_out):
    rows_first, rows_second, features = tokens.shape
    channels = w_in.shape[1]
    length_second = rows_second * n_c
    sizes = chunk_sizes(channels // GROUP, n_r)
    distinct = sorted(set(sizes))
    kinds = [distinct.index(size) for size in sizes]
    pieces = [Piece(size, n_r, n_c, rows_first, rows_second, length_second) for size in distinct]
    block, out_rows = pieces[0].block, pieces[0].out_rows
    rows = rows_first * rows_second
    tokens = tokens.transpose(1, 0, 2).reshape(rows, features)
    kind = jnp.bfloat16
    tables = []
    for piece in pieces:
        forward, back = channel_tables(piece, n_r)
        first, second = position_tables(piece, rows_first, rows_second, n_r, n_c)
        tables += [jnp.asarray(np.asarray(x, np.float32).astype(kind)) for x in (forward, first, second, back)]
    hbm = pl.BlockSpec(memory_space=pltpu.HBM)
    vmem = pl.BlockSpec(memory_space=pltpu.VMEM)
    dma = pltpu.SemaphoreType.DMA
    scratch = [
        pltpu.VMEM((rows, features), kind),
        pltpu.VMEM((features // LANES, LANES), kind),
        pltpu.VMEM((rows, features), kind),
        pltpu.VMEM(w_in.shape, kind),
    ]
    for p in range(len(pieces)):
        forward, first, second, back = tables[4 * p : 4 * p + 4]
        scratch += [pltpu.VMEM(x, kind) for x in (forward.shape, first.shape[1:], second.shape[1:], back.shape)]
    for p, piece in enumerate(pieces):
        count = kinds.count(p)
        for first_size, second_size in ((n_r, piece.rows1), (n_c, piece.rows2), (n_r, piece.rows3)):
            scratch += [pltpu.VMEM((count, first_size, second_size, LANES), kind)] * 2
    steps = len(kinds)
    scratch += [dma((2 + steps,)), dma((len(pieces), 4)), dma((3, steps))]
    scratch += [dma((steps, n)) for n in (n_r, n_r, n_c, n_c, n_r, n_r)]
    operands = (tokens, norm_gain.reshape(-1, LANES), w_in, *tables)
    spectrum = pl.pallas_call(
        functools.partial(kernel, n_r, n_c, pieces, kinds),
        out_shape=pltpu.VMEM((out_rows, channels), kind),
        in_specs=[hbm] * len(operands),
        out_specs=vmem,
        scratch_shapes=scratch,
        compiler_params=pltpu.CompilerParams(
            collective_id=0, has_side_effects=True, vmem_limit_bytes=53 * 1024 * 1024
        ),
    )(*[pltpu.with_memory_space_constraint(x, pltpu.HBM) for x in operands])
    return pl.pallas_call(
        last_product,
        out_shape=jax.ShapeDtypeStruct((length_second // n_r, block, features), kind),
        in_specs=[vmem] * 2,
        out_specs=vmem,
        compiler_params=pltpu.CompilerParams(vmem_limit_bytes=16 * 1024 * 1024),
    )(spectrum, w_out)


def fits(n_r, n_c, tokens_shape, channels):
    length_first, length_second, _ = tokens_shape
    return (
        n_r > 1
        and n_c & (n_c - 1) == 0
        and GROUP % (2 * n_r) == 0
        and length_first % (2 * n_c) == 0
        and SUBLANES % (length_first // n_c) == 0
        and length_first // n_r % ROWS == 0
        and length_second // n_r * (length_first // n_c) % ROWS == 0
        and length_second % n_r == 0
        and all(LANES % (size * GROUP // n_r) == 0 for size in chunk_sizes(channels // GROUP, n_r))
    )


def tables(length):
    series = jnp.arange(length, dtype=jnp.int32)
    product = series[:, None] * series[None, :] % length
    angles = product.astype(jnp.float32) * (2.0 * math.pi / length)
    return (jnp.cos(angles), jnp.sin(angles))


def folded_order(length_first, devices):
    block = length_first // devices
    half_block = block // 2
    series = jnp.arange(length_first, dtype=jnp.int32)
    device = series // block
    inner = series % block
    lower = device * half_block + inner
    upper = length_first - device * half_block - (inner - half_block)
    upper = jnp.where((device == 0) & (inner == half_block), length_first // 2, upper)
    return jnp.where(inner < half_block, lower, upper) % length_first


def to_channels(values, row_count):
    rows_first, rows_second, channels = values.shape
    width = channels // row_count
    parted = values.reshape(rows_first, rows_second, row_count, width).transpose(2, 0, 1, 3)
    return parted.reshape(row_count * rows_first, rows_second * width)


def product(table, values):
    return jnp.dot(table, values, precision=highest)


def middle(real_part, imag_part, width):
    length_first = real_part.shape[0]
    rows_second = real_part.shape[1] // width
    col_count = lax.axis_size("col")
    length_second = rows_second * col_count
    positions = length_first * length_second
    frequency = folded_order(length_first, col_count)
    series = jnp.arange(length_first, dtype=jnp.int32)
    first_angle = (frequency[:, None] * series[None, :] % length_first).astype(jnp.float32)
    first_angle = first_angle * (2.0 * math.pi / length_first)
    first_cos = jnp.cos(first_angle)
    first_sin = jnp.sin(first_angle)
    first_real = product(first_cos, real_part)
    first_imag = -product(first_sin, real_part)
    first_real = first_real + product(first_sin, imag_part)
    first_imag = first_imag + product(first_cos, imag_part)
    first_real = first_real.reshape(length_first, rows_second, width)
    first_imag = first_imag.reshape(length_first, rows_second, width)
    second_index = lax.axis_index("col") * rows_second + jnp.arange(rows_second, dtype=jnp.int32)
    twiddle_angle = (frequency[:, None] * second_index[None, :] % positions).astype(jnp.float32)
    twiddle_angle = twiddle_angle * (2.0 * math.pi / positions)
    twiddle_cos = jnp.cos(twiddle_angle)[:, :, None]
    twiddle_sin = jnp.sin(twiddle_angle)[:, :, None]
    turned_real = first_real * twiddle_cos + first_imag * twiddle_sin
    turned_imag = first_imag * twiddle_cos - first_real * twiddle_sin
    turned = jnp.stack([turned_real, turned_imag]).transpose(0, 2, 1, 3)
    turned = turned.reshape(2, rows_second, length_first * width)
    exchanged = lax.all_to_all(
        turned.astype(jnp.bfloat16), "col", split_axis=2, concat_axis=1, tiled=True
    ).astype(turned.dtype)
    second_cos, second_sin = tables(length_second)
    block = length_first // col_count
    out_shape = (length_second, block, width)
    out_real = (product(second_cos, exchanged[0]) + product(second_sin, exchanged[1])).reshape(
        out_shape
    )
    return out_real


def shards(tokens, norm_gain, w_in, w_out):
    rows_first, rows_second, features = tokens.shape
    row_count = lax.axis_size("row")
    length_first = rows_first * row_count
    length_second = rows_second * lax.axis_size("col")
    channels = w_in.shape[1]
    width = channels // row_count
    groups = channels // GROUP
    scaling = 1.0 / math.sqrt(length_first * length_second * GROUP)
    floats = tokens.astype(jnp.float32)
    normed = (
        floats
        * lax.rsqrt(jnp.mean(floats * floats, axis=-1, keepdims=True) + norm_eps)
        * norm_gain.astype(jnp.float32)
    ).astype(jnp.bfloat16)
    mapped = jnp.dot(normed.reshape(-1, features), w_in, preferred_element_type=jnp.float32)
    mapped = mapped.astype(jnp.bfloat16).reshape(rows_first, rows_second, channels)
    channel_cos, channel_sin = tables(GROUP)
    grouped = mapped.astype(jnp.float32).reshape(rows_first, rows_second, groups, GROUP)
    spec_real = jnp.einsum("abgj,jm->abgm", grouped, channel_cos, precision=highest)
    spec_imag = -jnp.einsum("abgj,jm->abgm", grouped, channel_sin, precision=highest)
    stacked = jnp.stack(
        [
            to_channels(spec_real.reshape(rows_first, rows_second, channels), row_count),
            to_channels(spec_imag.reshape(rows_first, rows_second, channels), row_count),
        ]
    )
    arrived = lax.all_to_all(
        stacked.astype(jnp.bfloat16), "row", split_axis=1, concat_axis=1, tiled=True
    ).astype(stacked.dtype)
    result = middle(arrived[0], arrived[1], width)
    spectrum = (result * scaling).astype(jnp.bfloat16)
    returned = lax.all_to_all(spectrum, "row", split_axis=0, concat_axis=2, tiled=True)
    mixed = jnp.dot(returned.reshape(-1, channels), w_out, preferred_element_type=jnp.float32)
    return mixed.astype(jnp.bfloat16).reshape(returned.shape[0], returned.shape[1], features)


def solution(mesh):
    in_specs = (P("row", "col", None), P(), P(), P())
    out_specs = P("row", "col", None)
    n_r, n_c = mesh.shape["row"], mesh.shape["col"]

    def run(tokens, norm_gain, w_in, w_out):
        whole = fits(n_r, n_c, tokens.shape, w_in.shape[1])
        body = functools.partial(fused_shards, n_r, n_c) if whole else shards
        return jax.shard_map(body, mesh=mesh, in_specs=in_specs, out_specs=out_specs, check_vma=False)(
            tokens, norm_gain, w_in, w_out
        )

    return run
```

time: 28.9 us -> 28.3 us (0.979)
  Pallas kernels: 28.7 us -> 28.2 us
    pallas_call x1, Pallas kernels: 26.9 us -> 26.3 us  [fused_shards(): pl.pallas_call(functools.partial(kernel, n_r, n_c, pieces, kinds), out_sh...]
where the time goes in v2:
time: 28.3 us; the launch traced here: 28.2 us
  Pallas kernels  28.2 us (100%)
    pallas_call x1, Pallas kernels, fused_shards(): pl.pallas_call(functools.partial(kernel, n_r, n_c, pieces, kinds), out_sh...  26.3 us
    pallas_call x1, Pallas kernels, fused_shards(): pl.pallas_call(last_product, out_shape=jax.ShapeDtypeStruct((length_secon...  1.86 us

profile of v2, /device:TPU:0, one launch (start us, length us, event | category | flops | bytes accessed | tf_op | source)
XLA Modules:
  0.0 28.2 jit_solution(841823814691380299)
XLA Ops:
  0.0 0.0 copy-start
  0.0 26.3 %shard_map.118.spectrum = bf16[144,1152]{1,0:T(8,128)(2,1)S(1)} custom-call(bf16[144,2048]{1,0:T(8,128)(2,1)} %bitcast.4, bf16[16,128]{1,0:T(8,128)(2,1)} %bitcast.5, bf16[2048,1152]{1,0:T(8,128)(2,1)} %refs_2_.1, bf16[512,512]{1,0:T(8,128)(2,1)} %constant.12.clone.refs_3_.refs_7_, bf16[8,768,160]{2,1,0:T(8,128)(2,1)} %constant.13.clone.refs_4_, ...), custom_call_target="tpu_custom_call" | custom-call | tf_op jit(solution)/shard_map/pallas_call | solution.py:408
  26.3 0.0 copy-done
  26.3 1.9 %shard_map.119 = bf16[36,4,2048]{2,1,0:T(4,128)(2,1)} custom-call(bf16[144,1152]{1,0:T(8,128)(2,1)S(1)} %shard_map.118.spectrum, bf16[1152,2048]{1,0:T(8,128)(2,1)S(1)} %copy-done), custom_call_target="tpu_custom_call" | custom-call | tf_op jit(solution)/shard_map/pallas_call | solution.py:418
Async XLA Ops:
  0.0 26.3 %copy-start = (bf16[1152,2048]{1,0:T(8,128)(2,1)S(1)}, bf16[1152,2048]{1,0:T(8,128)(2,1)}, u32[]{:S(2)}) copy-start(bf16[1152,2048]{1,0:T(8,128)(2,1)} %w_out.1) | copy-start | bytes 14155780

commit v3 on v2

--- a/solution.py
+++ b/solution.py
@@ -13,7 +13,10 @@
 LANES = 128
 SUBLANES = 16
 ROWS = 8
-LAG = 2
+LAG = 3
+TAIL = 2
+HELD = 3
+COLUMNS = 512
 MESH = pl.DeviceIdType.MESH
 
 
@@ -65,7 +68,7 @@
     width = GROUP // n_r
     half = width // 2
     j = np.arange(GROUP)
-    forward = np.zeros((piece.parts, piece.groups, GROUP, n_r, piece.parts, piece.groups, width))
+    forward = np.zeros((GROUP, n_r, width))
     back = np.zeros((n_r, piece.parts, piece.groups, width, piece.parts, piece.groups, GROUP))
     for row in range(n_r):
         for x in range(width):
@@ -78,13 +81,13 @@
                 entries = [(GROUP // 2, 1.0)]
             elif m:
                 entries = [(m, 1.0 if cosine else -1.0), (GROUP - m, 1.0)]
+            forward[:, row, x] = column
             for q in range(piece.parts):
                 for g in range(piece.groups):
-                    forward[q, g, :, row, q, g, x] = column
                     for at, sign in entries:
                         back[row, q, g, x, q, g, at] = sign
     size = piece.parts * piece.channels
-    return forward.reshape(size, n_r * LANES), back.reshape(n_r * LANES, size)
+    return forward.reshape(GROUP, LANES), back.reshape(n_r * LANES, size)
 
 
 def position_tables(piece, rows_first, rows_second, n_r, n_c):
@@ -159,6 +162,12 @@
     return places
 
 
+def origin_first(me, count):
+    places = far_first(me, count)
+    inside = (me > 0) & (me < count // 2)
+    return [jnp.where(inside, before, place) for before, place in zip([0] + places[:-1], places)]
+
+
 def kernel(n_r, n_c, pieces, kinds, *refs):
     refs = list(refs)
 
@@ -168,13 +177,14 @@
         return taken
 
     many = len(pieces)
-    tokens, gain, w_in = take(3)
-    tables_hbm = [take(4) for _ in pieces]
-    (out,) = take(1)
-    tok_v, gain_v, norm_v, win_v = take(4)
-    tables_v = [take(4) for _ in pieces]
+    tokens, gain, w_in, w_out = take(4)
+    (forward,) = take(1)
+    tables_hbm = [take(3) for _ in pieces]
+    partial, spectrum, tail_w = take(3)
+    tok_v, gain_v, norm_v, win_v, early_v, wout_v, forward_v = take(7)
+    tables_v = [take(3) for _ in pieces]
     buffers = [take(6) for _ in pieces]
-    load_sem, table_sem, self_sem, send1, recv1, send2, recv2, send3, recv3 = take(9)
+    load_sem, out_sem, table_sem, send_sem, recv_sem = take(5)
     row, col = lax.axis_index("row"), lax.axis_index("col")
     rows, features = tokens.shape
     steps = len(kinds)
@@ -192,29 +202,28 @@
         pl.semaphore_signal(barrier, inc=1, device_id={"col": bits_apart(col, d, n_c)}, device_id_type=MESH)
 
     load_tok = pltpu.make_async_copy(tokens, tok_v, load_sem.at[0])
+    load_forward = pltpu.make_async_copy(forward, forward_v, load_sem.at[2])
     load_gain = pltpu.make_async_copy(gain, gain_v, load_sem.at[1])
     load_win = [
-        pltpu.make_async_copy(w_in.at[:, lo:hi], win_v.at[:, lo:hi], load_sem.at[2 + t])
+        pltpu.make_async_copy(w_in.at[:, lo:hi], win_v.at[:, lo:hi], load_sem.at[3 + t])
         for t, (lo, hi) in enumerate(spans)
     ]
     load = []
-    for p, (forward, first, second, back) in enumerate(tables_hbm):
-        sources = (forward, first.at[col], second.at[jnp.minimum(col, 1)], back)
+    for p, (first, second, back) in enumerate(tables_hbm):
+        sources = (first.at[col], second.at[jnp.minimum(col, 1)], back)
         load.append(
             [pltpu.make_async_copy(x, y, table_sem.at[p, n]) for n, (x, y) in enumerate(zip(sources, tables_v[p]))]
         )
+    head = spans[steps - TAIL][0]
+    load_wout = [
+        pltpu.make_async_copy(w_out.at[:head], wout_v, out_sem.at[0]),
+        pltpu.make_async_copy(w_out.at[head:], tail_w, out_sem.at[1]),
+    ]
     load_tok.start()
     load_gain.start()
-    started = set()
-    for t, kind in enumerate(kinds):
-        load_win[t].start()
-        if kind not in started:
-            load[kind][0].start()
-            started.add(kind)
-    for n in (1, 2):
-        for p in range(many):
-            load[p][n].start()
-    pending = {(p, n) for p in range(many) for n in range(4)}
+    load_forward.start()
+    load_win[0].start()
+    pending = {(p, n) for p in range(many) for n in range(3)}
 
     def table(p, n):
         if (p, n) in pending:
@@ -224,99 +233,117 @@
 
     load_tok.wait()
     load_gain.wait()
-    floats = tok_v[...].astype(jnp.float32)
-    inverse = lax.rsqrt(jnp.mean(floats * floats, axis=-1, keepdims=True) + norm_eps)
     gains = gain_v[...].astype(jnp.float32)
+    squares = jnp.zeros((rows, LANES), jnp.float32)
     for at in range(features // LANES):
         lanes = slice(at * LANES, (at + 1) * LANES)
-        scaled = tok_v[:, lanes].astype(jnp.float32) * inverse * gains[at : at + 1, :]
-        norm_v[:, lanes] = scaled.astype(jnp.bfloat16)
+        floats = tok_v[:, lanes].astype(jnp.float32)
+        squares = squares + floats * floats
+        norm_v[:, lanes] = (floats * gains[at : at + 1, :]).astype(jnp.bfloat16)
+    inverse = lax.rsqrt(jnp.sum(squares, axis=-1, keepdims=True) / features + norm_eps)
 
     row_targets = far_first(row, n_r)
-    col_targets = [bits_apart(col, d, n_c) for d in range(n_c - 1, 0, -1)]
-    stages = (
-        (row, row_targets, send1, recv1, "row"),
-        (col, col_targets, send2, recv2, "col"),
-        (row, row_targets, send3, recv3, "row"),
-    )
-
-    def send(sent, came, stage, seat, t, target):
-        me, targets, send_sem, recv_sem, axis = stages[stage]
-        d = bits_apart(me, target, len(targets) + 1)
-        copy = pltpu.make_async_remote_copy(
-            src_ref=sent.at[seat, target],
-            dst_ref=came.at[seat, me],
-            send_sem=send_sem.at[t, d],
-            recv_sem=recv_sem.at[t, d],
-            device_id={axis: target},
-            device_id_type=MESH,
-        )
-        copy.start()
-        return copy
-
-    def keep(sent, came, stage, seat, t):
+    col_targets = [k + jnp.where(k >= col, 1, 0) for k in range(n_c - 1)]
+    stages = ((row, row_targets, "row"), (col, col_targets, "col"), (row, origin_first(row, n_r), "row"))
+
+    def exchange(stage, t, span=slice(None)):
+        p, seat = kinds[t], seats[t]
+        sent, came = buffers[p][2 * stage : 2 * stage + 2]
+        me, targets, axis = stages[stage]
+        for target in targets[span]:
+            pltpu.make_async_remote_copy(
+                src_ref=sent.at[seat, target],
+                dst_ref=came.at[seat, me],
+                send_sem=send_sem.at[stage, p],
+                recv_sem=recv_sem.at[stage, t],
+                device_id={axis: target},
+                device_id_type=MESH,
+            ).start()
+
+    def keep(stage, t):
+        p, seat = kinds[t], seats[t]
+        sent, came = buffers[p][2 * stage : 2 * stage + 2]
         me = stages[stage][0]
-        copy = pltpu.make_async_copy(sent.at[seat, me], came.at[seat, me], self_sem.at[stage, t])
-        copy.start()
-        return copy
-
-    def exchange(sent, came, stage, seat, t):
-        copies = [send(sent, came, stage, seat, t, target) for target in stages[stage][1]]
-        return copies + [keep(sent, came, stage, seat, t)]
+        pltpu.make_async_copy(sent.at[seat, me], came.at[seat, me], recv_sem.at[stage, t]).start()
+
+    def arrived(stage, t):
+        came = buffers[kinds[t]][2 * stage + 1].at[seats[t]]
+        pltpu.make_async_copy(came, came, recv_sem.at[stage, t]).wait()
+        return came
+
+    def all_sent():
+        for stage, (_, targets, _) in enumerate(stages):
+            for p in range(many):
+                gone = buffers[p][2 * stage].at[:, 0 : len(targets)]
+                pltpu.make_async_copy(gone, gone, send_sem.at[stage, p]).wait()
 
     lane = lax.broadcasted_iota(jnp.int32, (1, LANES), 1)
     turn = lane % (GROUP // n_r)
     cosine = (turn < GROUP // n_r // 2) | ((turn == GROUP // n_r // 2) & (row == 0))
-    copies1, copies2, copies3 = {}, {}, {}
 
     def start(t):
         p, seat = kinds[t], seats[t]
         piece = pieces[p]
         lo, hi = spans[t]
         load_win[t].wait()
-        mapped = jnp.dot(norm_v[...], win_v[:, lo:hi], preferred_element_type=jnp.float32)
+        if t == 0:
+            load_forward.wait()
+            for other in load_win[1:]:
+                other.start()
+            for n in range(2):
+                for other in sorted(range(many), key=kinds.index):
+                    load[other][n].start()
+        mapped = jnp.dot(norm_v[...], win_v[:, lo:hi], preferred_element_type=jnp.float32) * inverse
         short = piece.parts * piece.rows1 - rows
         if short:
             mapped = jnp.concatenate([mapped, jnp.zeros((short, hi - lo), jnp.float32)], axis=0)
-        blocks = [mapped[q * piece.rows1 : (q + 1) * piece.rows1] for q in range(piece.parts)]
-        side = jnp.concatenate(blocks, axis=1).astype(jnp.bfloat16)
-        turned = jnp.dot(side, table(p, 0)[...], preferred_element_type=jnp.float32).astype(jnp.bfloat16)
-        sent, came = buffers[p][:2]
+        blocks = [
+            mapped[q * piece.rows1 : (q + 1) * piece.rows1, g * GROUP : (g + 1) * GROUP]
+            for q in range(piece.parts)
+            for g in range(piece.groups)
+        ]
+        side = jnp.concatenate(blocks, axis=0).astype(jnp.bfloat16)
+        turned = jnp.dot(side, forward_v[...], preferred_element_type=jnp.float32)
+        sent = buffers[p][0]
+        width = GROUP // n_r
         for r in range(n_r):
-            sent[seat, r] = turned[:, r * LANES : (r + 1) * LANES]
+            total = None
+            for k in range(len(blocks)):
+                strip = turned[k * piece.rows1 : (k + 1) * piece.rows1]
+                if k != r:
+                    strip = pltpu.roll(strip, (k - r) * width % LANES, 1)
+                total = strip if total is None else jnp.where(lane < k * width, total, strip)
+            sent[seat, r] = total.astype(jnp.bfloat16)
         if t == 0:
             pl.semaphore_wait(barrier, n_r + n_c - 2)
-        copies1[t] = exchange(sent, came, 0, seat, t)
+        exchange(0, t)
+        keep(0, t)
 
     def middle_first(t):
         p, seat = kinds[t], seats[t]
         piece = pieces[p]
-        weights = table(p, 1)
-        for copy in copies1[t]:
-            copy.wait()
-        values = buffers[p][1][seat].reshape(n_r * piece.rows1, LANES)
+        weights = table(p, 0)
+        values = arrived(0, t)[...].reshape(n_r * piece.rows1, LANES)
         both = jnp.dot(weights[...], values, preferred_element_type=jnp.float32)
         size = n_c * piece.rows2
         total = both[:size]
         for q in range(1, piece.parts):
             total = jnp.where(lane < q * piece.used, total, both[q * size : (q + 1) * size])
-        sent, came = buffers[p][2:4]
-        sent[seat] = total.astype(jnp.bfloat16).reshape(n_c, piece.rows2, LANES)
-        copies2[t] = exchange(sent, came, 1, seat, t)
+        buffers[p][2][seat] = total.astype(jnp.bfloat16).reshape(n_c, piece.rows2, LANES)
+        exchange(1, t)
+        keep(1, t)
 
     def middle_second(t):
         p, seat = kinds[t], seats[t]
         piece = pieces[p]
-        weights = table(p, 2)
-        for copy in copies2[t]:
-            copy.wait()
-        values = buffers[p][3][seat].reshape(n_c * piece.rows2, LANES)
+        weights = table(p, 1)
+        values = arrived(1, t)[...].reshape(n_c * piece.rows2, LANES)
         floats = values.astype(jnp.float32)
         rolled = [values] + [
             pltpu.roll(floats, d * piece.used, 1).astype(jnp.bfloat16) for d in range(1, piece.parts)
         ]
         deep = jnp.concatenate(rolled, axis=0)
-        sent, came = buffers[p][4:6]
+        sent = buffers[p][4]
         size = piece.rows3
         for r in range(n_r):
             both = jnp.dot(weights[r], deep, preferred_element_type=jnp.float32)
@@ -328,44 +355,73 @@
             for q in range(1, piece.parts):
                 total = jnp.where(lane < q * piece.used, total, chosen[q])
             sent[seat, r] = total.astype(jnp.bfloat16)
-        copies3[t] = exchange(sent, came, 2, seat, t)
+        exchange(2, t, slice(0, 1))
+        if t < steps - HELD:
+            exchange(2, t, slice(1, None))
+        else:
+
+            @pl.when(row < n_r // 2)
+            def _():
+                exchange(2, t, slice(1, None))
+
+        if t == steps - 1:
+
+            @pl.when(row >= n_r // 2)
+            def _():
+                for held in range(steps - HELD, steps):
+                    exchange(2, held, slice(1, None))
+
+        keep(2, t)
 
     def finish(t):
         p, seat = kinds[t], seats[t]
         piece = pieces[p]
         lo, hi = spans[t]
-        weights = table(p, 3)
-        for copy in copies3[t]:
-            copy.wait()
-        side = jnp.concatenate([buffers[p][5][seat, r] for r in range(n_r)], axis=1)
+        weights = table(p, 2)
+        came = arrived(2, t)
+        side = jnp.concatenate([came[r] for r in range(n_r)], axis=1)
         total = jnp.dot(side, weights[...], preferred_element_type=jnp.float32).astype(jnp.bfloat16)
         size = piece.channels
+        place, lo = (early_v, lo) if t < steps - TAIL else (spectrum, lo - head)
         for q in range(piece.parts):
             above, below = q * piece.rows3, min(piece.out_rows, (q + 1) * piece.rows3)
-            out[above:below, lo:hi] = total[: below - above, q * size : (q + 1) * size]
+            place[above:below, lo : lo + size] = total[: below - above, q * size : (q + 1) * size]
+        if t == steps - TAIL - 1:
+            load_wout[0].wait()
+            for at in range(0, features, COLUMNS):
+                columns = slice(at, at + COLUMNS)
+                partial[:, columns] = jnp.dot(early_v[...], wout_v[:, columns], preferred_element_type=jnp.float32)
+            load_wout[1].wait()
 
     for t in range(steps):
         start(t)
     for p in range(many):
-        load[p][3].start()
+        load[p][2].start()
+    for copy in load_wout:
+        copy.start()
     for job, t in schedule(steps):
         (middle_first, middle_second, finish)[job](t)
+    all_sent()
 
 
 def schedule(steps):
-    jobs, ready = [], 0
-    for t in range(steps):
-        jobs.append((0, t))
-        while ready <= t - LAG:
-            jobs.append((1, ready))
-            ready += 1
-    jobs += [(1, t) for t in range(ready, steps)]
-    return jobs + [(2, t) for t in range(steps)]
-
-
-def last_product(spectrum, w_out, out):
-    total = jnp.dot(spectrum[...], w_out[...], preferred_element_type=jnp.float32)
-    out[...] = total.reshape(out.shape).astype(jnp.bfloat16)
+    jobs = [(0, t) for t in range(steps)]
+    jobs[min(LAG, steps) : min(LAG, steps)] = [(1, 0)]
+    return jobs + [(1, t) for t in range(1, steps)] + [(2, t) for t in range(steps)]
+
+
+def last_product(partial, spectrum, w_tail, out, out_v, sems):
+    copies = []
+    for n, at in enumerate(range(0, partial.shape[1], COLUMNS)):
+        columns = slice(at, at + COLUMNS)
+        total = jnp.dot(spectrum[...], w_tail[:, columns], preferred_element_type=jnp.float32)
+        total = total + partial[:, columns]
+        out_v[:, :, columns] = total.reshape(*out_v.shape[:2], COLUMNS).astype(jnp.bfloat16)
+        copy = pltpu.make_async_copy(out_v.at[:, :, columns], out.at[:, :, columns], sems.at[n])
+        copy.start()
+        copies.append(copy)
+    for copy in copies:
+        copy.wait()
 
 
 def fused_shards(n_r, n_c, tokens, norm_gain, w_in, w_out):
@@ -377,14 +433,16 @@
     kinds = [distinct.index(size) for size in sizes]
     pieces = [Piece(size, n_r, n_c, rows_first, rows_second, length_second) for size in distinct]
     block, out_rows = pieces[0].block, pieces[0].out_rows
+    head = sum(sizes[:-TAIL]) * GROUP
     rows = rows_first * rows_second
     tokens = tokens.transpose(1, 0, 2).reshape(rows, features)
     kind = jnp.bfloat16
-    tables = []
+    tables = [channel_tables(pieces[0], n_r)[0]]
     for piece in pieces:
-        forward, back = channel_tables(piece, n_r)
+        _, back = channel_tables(piece, n_r)
         first, second = position_tables(piece, rows_first, rows_second, n_r, n_c)
-        tables += [jnp.asarray(np.asarray(x, np.float32).astype(kind)) for x in (forward, first, second, back)]
+        tables += [first, second, back]
+    tables = [jnp.asarray(np.asarray(x, np.float32).astype(kind)) for x in tables]
     hbm = pl.BlockSpec(memory_space=pltpu.HBM)
     vmem = pl.BlockSpec(memory_space=pltpu.VMEM)
     dma = pltpu.SemaphoreType.DMA
@@ -393,39 +451,47 @@
         pltpu.VMEM((features // LANES, LANES), kind),
         pltpu.VMEM((rows, features), kind),
         pltpu.VMEM(w_in.shape, kind),
+        pltpu.VMEM((out_rows, head), kind),
+        pltpu.VMEM((head, features), kind),
+        pltpu.VMEM(tables[0].shape, kind),
     ]
     for p in range(len(pieces)):
-        forward, first, second, back = tables[4 * p : 4 * p + 4]
-        scratch += [pltpu.VMEM(x, kind) for x in (forward.shape, first.shape[1:], second.shape[1:], back.shape)]
+        first, second, back = tables[3 * p + 1 : 3 * p + 4]
+        scratch += [pltpu.VMEM(x, kind) for x in (first.shape[1:], second.shape[1:], back.shape)]
     for p, piece in enumerate(pieces):
         count = kinds.count(p)
         for first_size, second_size in ((n_r, piece.rows1), (n_c, piece.rows2), (n_r, piece.rows3)):
             scratch += [pltpu.VMEM((count, first_size, second_size, LANES), kind)] * 2
     steps = len(kinds)
-    scratch += [dma((2 + steps,)), dma((len(pieces), 4)), dma((3, steps))]
-    scratch += [dma((steps, n)) for n in (n_r, n_r, n_c, n_c, n_r, n_r)]
-    operands = (tokens, norm_gain.reshape(-1, LANES), w_in, *tables)
-    spectrum = pl.pallas_call(
+    scratch += [dma((3 + steps,)), dma((2,)), dma((len(pieces), 3)), dma((3, len(pieces))), dma((3, steps))]
+    operands = (tokens, norm_gain.reshape(-1, LANES), w_in, w_out, *tables)
+    partial, spectrum, w_tail = pl.pallas_call(
         functools.partial(kernel, n_r, n_c, pieces, kinds),
-        out_shape=pltpu.VMEM((out_rows, channels), kind),
+        out_shape=[
+            pltpu.VMEM((out_rows, features), jnp.float32),
+            pltpu.VMEM((out_rows, channels - head), kind),
+            pltpu.VMEM((channels - head, features), kind),
+        ],
         in_specs=[hbm] * len(operands),
-        out_specs=vmem,
+        out_specs=[vmem] * 3,
         scratch_shapes=scratch,
         compiler_params=pltpu.CompilerParams(
             collective_id=0, has_side_effects=True, vmem_limit_bytes=53 * 1024 * 1024
         ),
     )(*[pltpu.with_memory_space_constraint(x, pltpu.HBM) for x in operands])
+    out_shape = (length_second // n_r, block, features)
     return pl.pallas_call(
         last_product,
-        out_shape=jax.ShapeDtypeStruct((length_second // n_r, block, features), kind),
-        in_specs=[vmem] * 2,
-        out_specs=vmem,
+        out_shape=jax.ShapeDtypeStruct(out_shape, kind),
+        in_specs=[vmem] * 3,
+        out_specs=hbm,
+        scratch_shapes=[pltpu.VMEM(out_shape, kind), dma((features // COLUMNS,))],
         compiler_params=pltpu.CompilerParams(vmem_limit_bytes=16 * 1024 * 1024),
-    )(spectrum, w_out)
+    )(partial, spectrum, w_tail)
 
 
 def fits(n_r, n_c, tokens_shape, channels):
-    length_first, length_second, _ = tokens_shape
+    length_first, length_second, features = tokens_shape
     return (
         n_r > 1
         and n_c & (n_c - 1) == 0
@@ -435,6 +501,8 @@
         and length_first // n_r % ROWS == 0
         and length_second // n_r * (length_first // n_c) % ROWS == 0
         and length_second % n_r == 0
+        and features % COLUMNS == 0
+        and len(chunk_sizes(channels // GROUP, n_r)) > TAIL
         and all(LANES % (size * GROUP // n_r) == 0 for size in chunk_sizes(channels // GROUP, n_r))
     )
 

time: 28.3 us -> 25.4 us (0.90)
  Pallas kernels: 28.2 us -> 25.2 us
    pallas_call x1, Pallas kernels: 26.3 us -> 24 us  [fused_shards(): pl.pallas_call(functools.partial(kernel, n_r, n_c, pieces, kinds), out_sh...]
    pallas_call x1, Pallas kernels: 1.86 us -> 1.22 us  [fused_shards(): pl.pallas_call(last_product, out_shape=jax.ShapeDtypeStruct(out_shape, ki...]
where the time goes in v3:
time: 25.4 us; the launch traced here: 25.2 us
  Pallas kernels  25.2 us (99%)
    pallas_call x1, Pallas kernels, fused_shards(): pl.pallas_call(functools.partial(kernel, n_r, n_c, pieces, kinds), out_sh...  24 us
    pallas_call x1, Pallas kernels, fused_shards(): pl.pallas_call(last_product, out_shape=jax.ShapeDtypeStruct(out_shape, ki...  1.22 us

profile of v3, /device:TPU:0, one launch (start us, length us, event | category | flops | bytes accessed | tf_op | source)
XLA Modules:
  0.0 25.2 jit_solution(14046977027624438869)
XLA Ops:
  0.0 24.0 %shard_map.109 = (f32[144,2048]{1,0:T(8,128)S(1)}, bf16[144,384]{1,0:T(8,128)(2,1)S(1)}, bf16[384,2048]{1,0:T(8,128)(2,1)S(1)}) custom-call(bf16[144,2048]{1,0:T(8,128)(2,1)} %bitcast.4, bf16[16,128]{1,0:T(8,128)(2,1)} %bitcast.5, bf16[2048,1152]{1,0:T(8,128)(2,1)} %refs_2_.1, bf16[1152,2048]{1,0:T(8,128)(2,1)} %refs_3_.1, ...), custom_call_target="tpu_custom_call" | custom-call | tf_op jit(solution)/shard_map/pallas_call | solution.py:468
  24.0 1.2 %shard_map.110 = bf16[36,4,2048]{2,1,0:T(4,128)(2,1)} custom-call(f32[144,2048]{1,0:T(8,128)S(1)} %get-tuple-element.8.partial, bf16[144,384]{1,0:T(8,128)(2,1)S(1)} %get-tuple-element.9.spectrum, bf16[384,2048]{1,0:T(8,128)(2,1)S(1)} %get-tuple-element.10.w_tail), custom_call_target="tpu_custom_call" | custom-call | tf_op jit(solution)/shard_map/pallas_call | solution.py:483

commit v4 on v3

--- a/solution.py
+++ b/solution.py
@@ -55,7 +55,14 @@
         self.rows1 = self.seconds * rows_first
         self.rows2 = ceil_to(self.seconds * self.block, ROWS)
         self.out_rows = length_second // n_r * self.block
-        self.rows3 = ceil_to(-(-self.out_rows // self.parts), ROWS)
+        self.half = self.block // 2
+        self.strips = self.parts // self.half
+        self.step = self.out_rows // self.half // max(1, self.strips)
+        self.rows3 = ceil_to(self.step, ROWS)
+        depth = 2 * self.seconds
+        ends = [(f * depth // ROWS * ROWS, ceil_to((f + 1) * depth, ROWS)) for f in range(self.half)]
+        self.window = max(hi - lo for lo, hi in ends)
+        self.lows = [min(lo, self.rows2 - self.window) for lo, _ in ends]
 
 
 def chunk_sizes(groups, n_r):
@@ -97,11 +104,10 @@
     block, parts, seconds = piece.block, piece.parts, piece.seconds
     half = block // 2
     a = np.arange(length_first)
-    first = np.zeros((n_c, parts, n_c, piece.rows2, n_r, seconds, rows_first))
+    first = np.zeros((n_c, n_c, piece.rows2, n_r, seconds, rows_first))
     for col in range(n_c):
-        for i in range(rows_second):
-            q, j = divmod(i, seconds)
-            p = a * length_second + col * rows_second + i
+        for j in range(seconds):
+            p = a * length_second + col * rows_second + j
             for target in range(n_c):
                 for f_at in range(half):
                     f = target * half + f_at
@@ -109,8 +115,8 @@
                     real, imag = np.cos(angle), -np.sin(angle)
                     if f == 0:
                         real, imag = np.ones(length_first), (-1.0) ** a
-                    first[col, q, target, j * block + 2 * f_at, :, j, :] = real.reshape(n_r, rows_first)
-                    first[col, q, target, j * block + 2 * f_at + 1, :, j, :] = imag.reshape(n_r, rows_first)
+                    first[col, target, 2 * (f_at * seconds + j), :, j, :] = real.reshape(n_r, rows_first)
+                    first[col, target, 2 * (f_at * seconds + j) + 1, :, j, :] = imag.reshape(n_r, rows_first)
     k_b = np.arange(length_second)
     plain = np.zeros((2, 2, length_second, block, parts, n_c, piece.rows2))
     for other in range(2):
@@ -120,7 +126,8 @@
                     b = source * rows_second + i
                     f_at, upper = s % half, s >= half
                     q, j = divmod(i, seconds)
-                    re_at, im_at = (q, source, j * block + 2 * f_at), (q, source, j * block + 2 * f_at + 1)
+                    at = 2 * (f_at * seconds + j)
+                    re_at, im_at = (q, source, at), (q, source, at + 1)
                     if other == 0 and f_at == 0:
                         shift = length_first // 2 if upper else 0
                         angle = 2 * np.pi * (b * (k_b * length_first + shift) % positions) / positions
@@ -134,15 +141,28 @@
                     plain[(other, 0, slice(None), s) + im_at] = np.sin(angle) * sign
                     plain[(other, 1, slice(None), s) + re_at] = np.sin(angle)
                     plain[(other, 1, slice(None), s) + im_at] = -np.cos(angle) * sign
-    plain = plain.reshape(2, 2, n_r, piece.out_rows, parts, n_c * piece.rows2) / math.sqrt(positions * GROUP)
-    second = np.zeros((2, n_r, parts, 2, piece.rows3, parts, n_c * piece.rows2))
-    for q in range(parts):
-        lo, hi = q * piece.rows3, min(piece.out_rows, (q + 1) * piece.rows3)
-        for d in range(parts):
-            values = plain[:, :, :, lo:hi, (q - d) % parts]
-            second[:, :, q, :, : hi - lo, d] = values.transpose(0, 2, 1, 3, 4)
-    first = first.reshape(n_c, parts * n_c * piece.rows2, n_r * piece.rows1)
-    return first, second.reshape(2, n_r, parts * 2 * piece.rows3, parts * n_c * piece.rows2)
+    plain = plain.reshape(2, 2, n_r, piece.out_rows, parts, n_c, piece.rows2) / math.sqrt(positions * GROUP)
+    strips, step, window = piece.strips, piece.step, piece.window
+    second = np.zeros((n_c, half, n_r, strips, 2, piece.rows3, parts, n_c, window))
+    for col in range(n_c):
+        mine = plain[min(col, 1)].copy()
+        for f_at in range(half):
+            f = col * half + f_at
+            for q in range(parts if f else 0):
+                turn = 2 * np.pi * (f * q * seconds % positions) / positions
+                lo, hi = 2 * f_at * seconds, 2 * (f_at + 1) * seconds
+                real, imag = mine[..., q, :, lo:hi:2].copy(), mine[..., q, :, lo + 1 : hi : 2].copy()
+                mine[..., q, :, lo:hi:2] = real * np.cos(turn) - imag * np.sin(turn)
+                mine[..., q, :, lo + 1 : hi : 2] = real * np.sin(turn) + imag * np.cos(turn)
+        for f in range(half):
+            low = piece.lows[f]
+            for h in range(strips):
+                rows = half * (h * step + np.arange(step)) + f
+                for d in range(parts):
+                    values = mine[:, :, rows, (f * strips + h - d) % parts, :, low : low + window]
+                    second[col, f, :, h, :, :step, d] = values.transpose(1, 0, 2, 3, 4)
+    first = first.reshape(n_c, n_c * piece.rows2, n_r * piece.rows1)
+    return first, second.reshape(n_c, half, n_r * strips * 2 * piece.rows3, parts * n_c * window)
 
 
 def bits_apart(one, other, count):
@@ -181,7 +201,7 @@
     (forward,) = take(1)
     tables_hbm = [take(3) for _ in pieces]
     partial, spectrum, tail_w = take(3)
-    tok_v, gain_v, norm_v, win_v, early_v, wout_v, forward_v = take(7)
+    tok_v, gain_v, norm_v, win_v, early_v, wout_v, forward_v, woven_v = take(8)
     tables_v = [take(3) for _ in pieces]
     buffers = [take(6) for _ in pieces]
     load_sem, out_sem, table_sem, send_sem, recv_sem = take(5)
@@ -210,7 +230,7 @@
     ]
     load = []
     for p, (first, second, back) in enumerate(tables_hbm):
-        sources = (first.at[col], second.at[jnp.minimum(col, 1)], back)
+        sources = (first.at[col], second.at[col], back)
         load.append(
             [pltpu.make_async_copy(x, y, table_sem.at[p, n]) for n, (x, y) in enumerate(zip(sources, tables_v[p]))]
         )
@@ -324,11 +344,7 @@
         piece = pieces[p]
         weights = table(p, 0)
         values = arrived(0, t)[...].reshape(n_r * piece.rows1, LANES)
-        both = jnp.dot(weights[...], values, preferred_element_type=jnp.float32)
-        size = n_c * piece.rows2
-        total = both[:size]
-        for q in range(1, piece.parts):
-            total = jnp.where(lane < q * piece.used, total, both[q * size : (q + 1) * size])
+        total = jnp.dot(weights[...], values, preferred_element_type=jnp.float32)
         buffers[p][2][seat] = total.astype(jnp.bfloat16).reshape(n_c, piece.rows2, LANES)
         exchange(1, t)
         keep(1, t)
@@ -337,23 +353,24 @@
         p, seat = kinds[t], seats[t]
         piece = pieces[p]
         weights = table(p, 1)
-        values = arrived(1, t)[...].reshape(n_c * piece.rows2, LANES)
-        floats = values.astype(jnp.float32)
-        rolled = [values] + [
-            pltpu.roll(floats, d * piece.used, 1).astype(jnp.bfloat16) for d in range(1, piece.parts)
-        ]
-        deep = jnp.concatenate(rolled, axis=0)
+        values = arrived(1, t)
         sent = buffers[p][4]
         size = piece.rows3
+        count = n_c * piece.window
+        chosen = []
+        for f, low in enumerate(piece.lows):
+            floats = values[:, low : low + piece.window].reshape(count, LANES).astype(jnp.float32)
+            rolled = [floats] + [pltpu.roll(floats, d * piece.used, 1) for d in range(1, piece.parts)]
+            deep = jnp.concatenate([part.astype(jnp.bfloat16) for part in rolled], axis=0)
+            both = jnp.dot(weights[f], deep, preferred_element_type=jnp.float32)
+            blocks = [both[n * size : (n + 1) * size] for n in range(2 * n_r * piece.strips)]
+            chosen.append([jnp.where(cosine, *blocks[n : n + 2]) for n in range(0, len(blocks), 2)])
         for r in range(n_r):
-            both = jnp.dot(weights[r], deep, preferred_element_type=jnp.float32)
-            chosen = [
-                jnp.where(cosine, both[2 * q * size : (2 * q + 1) * size], both[(2 * q + 1) * size : (2 * q + 2) * size])
-                for q in range(piece.parts)
-            ]
-            total = chosen[0]
-            for q in range(1, piece.parts):
-                total = jnp.where(lane < q * piece.used, total, chosen[q])
+            total = None
+            for q in range(piece.parts):
+                f, h = divmod(q, piece.strips)
+                part = chosen[f][r * piece.strips + h]
+                total = part if total is None else jnp.where(lane < q * piece.used, total, part)
             sent[seat, r] = total.astype(jnp.bfloat16)
         exchange(2, t, slice(0, 1))
         if t < steps - HELD:
@@ -380,12 +397,16 @@
         weights = table(p, 2)
         came = arrived(2, t)
         side = jnp.concatenate([came[r] for r in range(n_r)], axis=1)
-        total = jnp.dot(side, weights[...], preferred_element_type=jnp.float32).astype(jnp.bfloat16)
-        size = piece.channels
+        total = jnp.dot(side, weights[...], preferred_element_type=jnp.float32)
+        size, step = piece.channels, piece.step
         place, lo = (early_v, lo) if t < steps - TAIL else (spectrum, lo - head)
         for q in range(piece.parts):
-            above, below = q * piece.rows3, min(piece.out_rows, (q + 1) * piece.rows3)
-            place[above:below, lo : lo + size] = total[: below - above, q * size : (q + 1) * size]
+            f, h = divmod(q, piece.strips)
+            for c in range(size // LANES):
+                at = q * size + c * LANES
+                woven_v[c, pl.ds(piece.half * h * step + f, step, stride=piece.half), :] = total[:step, at : at + LANES]
+        for c in range(size // LANES):
+            place[:, lo + c * LANES : lo + (c + 1) * LANES] = woven_v[c].astype(jnp.bfloat16)
         if t == steps - TAIL - 1:
             load_wout[0].wait()
             for at in range(0, features, COLUMNS):
@@ -454,6 +475,7 @@
         pltpu.VMEM((out_rows, head), kind),
         pltpu.VMEM((head, features), kind),
         pltpu.VMEM(tables[0].shape, kind),
+        pltpu.VMEM((max(sizes) * GROUP // LANES, out_rows, LANES), jnp.float32),
     ]
     for p in range(len(pieces)):
         first, second, back = tables[3 * p + 1 : 3 * p + 4]
@@ -490,6 +512,12 @@
     )(partial, spectrum, w_tail)
 
 
+def divided(n_r, n_c, length_first, length_second, size):
+    used, half = size * GROUP // n_r, length_first // n_c // 2
+    out_rows = length_second // n_r * 2 * half
+    return LANES % (used * half) == 0 and out_rows % (LANES // used) == 0
+
+
 def fits(n_r, n_c, tokens_shape, channels):
     length_first, length_second, features = tokens_shape
     return (
@@ -503,7 +531,7 @@
         and length_second % n_r == 0
         and features % COLUMNS == 0
         and len(chunk_sizes(channels // GROUP, n_r)) > TAIL
-        and all(LANES % (size * GROUP // n_r) == 0 for size in chunk_sizes(channels // GROUP, n_r))
+        and all(divided(n_r, n_c, length_first, length_second, size) for size in chunk_sizes(channels // GROUP, n_r))
     )
 
 

time: 25.4 us -> 25.3 us (level)
  no operation moved by 1% of the time
where the time goes in v4:
time: 25.3 us; the launch traced here: 25.2 us
  Pallas kernels  25.2 us (100%)
    pallas_call x1, Pallas kernels, fused_shards(): pl.pallas_call(functools.partial(kernel, n_r, n_c, pieces, kinds), out_sh...  24 us
    pallas_call x1, Pallas kernels, fused_shards(): pl.pallas_call(last_product, out_shape=jax.ShapeDtypeStruct(out_shape, ki...  1.21 us

profile of v4, /device:TPU:0, one launch (start us, length us, event | category | flops | bytes accessed | tf_op | source)
XLA Modules:
  0.0 25.2 jit_solution(9417883394010732299)
XLA Ops:
  0.0 24.0 %shard_map.109 = (f32[144,2048]{1,0:T(8,128)S(1)}, bf16[144,384]{1,0:T(8,128)(2,1)S(1)}, bf16[384,2048]{1,0:T(8,128)(2,1)S(1)}) custom-call(bf16[144,2048]{1,0:T(8,128)(2,1)} %bitcast.4, bf16[16,128]{1,0:T(8,128)(2,1)} %bitcast.5, bf16[2048,1152]{1,0:T(8,128)(2,1)} %refs_2_.1, bf16[1152,2048]{1,0:T(8,128)(2,1)} %refs_3_.1, ...), custom_call_target="tpu_custom_call" | custom-call | tf_op jit(solution)/shard_map/pallas_call | solution.py:490
  24.0 1.2 %shard_map.110 = bf16[36,4,2048]{2,1,0:T(4,128)(2,1)} custom-call(f32[144,2048]{1,0:T(8,128)S(1)} %get-tuple-element.8.partial, bf16[144,384]{1,0:T(8,128)(2,1)S(1)} %get-tuple-element.9.spectrum, bf16[384,2048]{1,0:T(8,128)(2,1)S(1)} %get-tuple-element.10.w_tail), custom_call_target="tpu_custom_call" | custom-call | tf_op jit(solution)/shard_map/pallas_call | solution.py:505

commit v5 on v4

--- a/solution.py
+++ b/solution.py
@@ -13,7 +13,7 @@
 LANES = 128
 SUBLANES = 16
 ROWS = 8
-LAG = 3
+LAG = 4
 TAIL = 2
 HELD = 3
 COLUMNS = 512
@@ -204,7 +204,7 @@
     tok_v, gain_v, norm_v, win_v, early_v, wout_v, forward_v, woven_v = take(8)
     tables_v = [take(3) for _ in pieces]
     buffers = [take(6) for _ in pieces]
-    load_sem, out_sem, table_sem, send_sem, recv_sem = take(5)
+    load_sem, send_sem, recv_sem = take(3)
     row, col = lax.axis_index("row"), lax.axis_index("col")
     rows, features = tokens.shape
     steps = len(kinds)
@@ -232,12 +232,15 @@
     for p, (first, second, back) in enumerate(tables_hbm):
         sources = (first.at[col], second.at[col], back)
         load.append(
-            [pltpu.make_async_copy(x, y, table_sem.at[p, n]) for n, (x, y) in enumerate(zip(sources, tables_v[p]))]
+            [
+                pltpu.make_async_copy(x, y, load_sem.at[2 * p + n if n < 2 else 4 + p])
+                for n, (x, y) in enumerate(zip(sources, tables_v[p]))
+            ]
         )
     head = spans[steps - TAIL][0]
     load_wout = [
-        pltpu.make_async_copy(w_out.at[:head], wout_v, out_sem.at[0]),
-        pltpu.make_async_copy(w_out.at[head:], tail_w, out_sem.at[1]),
+        pltpu.make_async_copy(w_out.at[:head], wout_v, load_sem.at[6]),
+        pltpu.make_async_copy(w_out.at[head:], tail_w, load_sem.at[7]),
     ]
     load_tok.start()
     load_gain.start()
@@ -485,7 +488,7 @@
         for first_size, second_size in ((n_r, piece.rows1), (n_c, piece.rows2), (n_r, piece.rows3)):
             scratch += [pltpu.VMEM((count, first_size, second_size, LANES), kind)] * 2
     steps = len(kinds)
-    scratch += [dma((3 + steps,)), dma((2,)), dma((len(pieces), 3)), dma((3, len(pieces))), dma((3, steps))]
+    scratch += [dma((max(8, 3 + steps),)), dma((3, len(pieces))), dma((3, steps))]
     operands = (tokens, norm_gain.reshape(-1, LANES), w_in, w_out, *tables)
     partial, spectrum, w_tail = pl.pallas_call(
         functools.partial(kernel, n_r, n_c, pieces, kinds),

time: 25.3 us -> 25.2 us (level)
  no operation moved by 1% of the time
where the time goes in v5:
time: 25.2 us; the launch traced here: 25 us
  Pallas kernels  25 us (99%)
    pallas_call x1, Pallas kernels, fused_shards(): pl.pallas_call(functools.partial(kernel, n_r, n_c, pieces, kinds), out_sh...  23.8 us
    pallas_call x1, Pallas kernels, fused_shards(): pl.pallas_call(last_product, out_shape=jax.ShapeDtypeStruct(out_shape, ki...  1.21 us

profile of v5, /device:TPU:0, one launch (start us, length us, event | category | flops | bytes accessed | tf_op | source)
XLA Modules:
  0.0 25.0 jit_solution(14501442473706295445)
XLA Ops:
  0.0 23.8 %shard_map.109 = (f32[144,2048]{1,0:T(8,128)S(1)}, bf16[144,384]{1,0:T(8,128)(2,1)S(1)}, bf16[384,2048]{1,0:T(8,128)(2,1)S(1)}) custom-call(bf16[144,2048]{1,0:T(8,128)(2,1)} %bitcast.4, bf16[16,128]{1,0:T(8,128)(2,1)} %bitcast.5, bf16[2048,1152]{1,0:T(8,128)(2,1)} %refs_2_.1, bf16[1152,2048]{1,0:T(8,128)(2,1)} %refs_3_.1, ...), custom_call_target="tpu_custom_call" | custom-call | tf_op jit(solution)/shard_map/pallas_call | solution.py:493
  23.8 1.2 %shard_map.110 = bf16[36,4,2048]{2,1,0:T(4,128)(2,1)} custom-call(f32[144,2048]{1,0:T(8,128)S(1)} %get-tuple-element.8.partial, bf16[144,384]{1,0:T(8,128)(2,1)S(1)} %get-tuple-element.9.spectrum, bf16[384,2048]{1,0:T(8,128)(2,1)S(1)} %get-tuple-element.10.w_tail), custom_call_target="tpu_custom_call" | custom-call | tf_op jit(solution)/shard_map/pallas_call | solution.py:508
